TPU v7x, 256 devices: a 4x2x16 block of a 4x16x16 slice. The times are simulated.
256 devices in a mesh: grp: 2 (over y), fs: 16 (over z), tp: 8 (over x, core).
Axes of the slice: x: 4, y: 2, z: 16, core: 2. Of those that a mesh axis runs over, the one named last changes fastest.
The devices are a block of a 4x16x16 slice.
Arguments:
- tokens: bfloat16 [16384, 2048], P(('grp', 'fs'), 'tp'), parts along dimension 0, may hold values from -16 to 16
- attn_gain: float32 [2048], replicated, may hold values from 0.1 to 1.9
- w_query: bfloat16 [2048, 1024], P('fs', 'tp'), may hold values from -0.125 to 0.125
- w_key: bfloat16 [2048, 1024], P('fs', 'tp'), may hold values from -0.125 to 0.125
- w_value: bfloat16 [2048, 2048], P('fs', 'tp'), may hold values from -0.125 to 0.125
- w_low: bfloat16 [2048, 32], replicated, may hold values from -0.125 to 0.125
- w_lift: bfloat16 [32, 1024], P(None, 'tp'), may hold values from -1 to 1
- decay_bias: float32 [1024], P('tp'), may hold values from -0.5 to 6
- head_gain: float32 [256], replicated, may hold values from 0.1 to 1.9
- w_out: bfloat16 [2048, 2048], P('tp', 'fs'), may hold values from -0.125 to 0.125
- ffn_gain: float32 [2048], replicated, may hold values from 0.1 to 1.9
- w_gate: bfloat16 [2048, 5632], P('fs', 'tp'), may hold values from -0.125 to 0.125
- w_up: bfloat16 [2048, 5632], P('fs', 'tp'), may hold values from -0.125 to 0.125
- w_down: bfloat16 [5632, 2048], P('tp', 'fs'), may hold values from -0.078125 to 0.078125
- final_gain: float32 [2048], P('tp'), may hold values from 0.1 to 1.9
Outputs:
- result: bfloat16 [16384, 2048], P(('grp', 'fs'), 'tp'), parts along dimension 0
There are 2 independent parts, one for each index of `grp`. A program takes and returns all parts, laid end to end along the dimension named above; an argument that names none is the same for every part. Nothing has to cross between parts.
All inputs are finite; a program needn't handle non-finite values.
Results may differ from a plain program's by a relative error of at most 0.015.
Values may be sent and summed in bfloat16 or wider, within the bound.
A program may use at most 64 MiB of HBM per device.

v0:
```python
import jax
import jax.numpy as jnp
from jax import lax
from jax.sharding import PartitionSpec as P

D = 2048
DK = 128
DV = 256
BLOCK = 64


epsilon = 1e-06
highest = lax.Precision.HIGHEST


def copy_for_each(x, axis):
    copies = jnp.broadcast_to(x, (lax.axis_size(axis), *x.shape))
    return lax.all_to_all(copies, axis, split_axis=0, concat_axis=0, tiled=True)


def laid_out(blocks, dim):
    blocks = jnp.moveaxis(blocks, 0, dim)
    shape = blocks.shape
    return blocks.reshape(*shape[:dim], shape[dim] * shape[dim + 1], *shape[dim + 2 :])


def gather_directly(x, axis, dim):
    blocks = copy_for_each(x, axis)
    return laid_out(blocks, dim)


def side_by_side(arrays, axis, dim, along):
    ends, at = ([], 0)
    for a in arrays[:-1]:
        at += a.shape[along]
        ends.append(at)
    both = jnp.concatenate(arrays, axis=along)
    return tuple(jnp.split(lax.all_gather(both, axis, axis=dim, tiled=True), ends, axis=along))


def in_blocks(x, dim, devices):
    before, after = (x.shape[:dim], x.shape[dim + 1 :])
    return jnp.moveaxis(x.reshape(*before, devices, -1, *after), dim, 0)


def summed_on_arrival(x, axis, dim):
    blocks = in_blocks(x, dim, lax.axis_size(axis))
    arrived = lax.all_to_all(blocks, axis, split_axis=0, concat_axis=0, tiled=True)
    return arrived.astype(jnp.float32).sum(axis=0)


def over_copies(x, axis):
    everything = copy_for_each(x, axis)
    return jnp.sum(everything, axis=0)


def rms_rows(values, gain):
    values = values.astype(jnp.float32)
    factor = lax.rsqrt(jnp.mean(values * values, axis=-1, keepdims=True) + epsilon)
    return values * factor * gain


def blockwise_gla(query_rows, key_rows, value_rows, log_decay, head_count):
    length = query_rows.shape[0]
    blocks = length // BLOCK

    def split_heads(array, depth):
        return (
            array.astype(jnp.float32)
            .reshape(blocks, BLOCK, head_count, depth)
            .transpose(2, 0, 1, 3)
        )

    query_f = split_heads(query_rows, DK) * DK ** (-0.5)
    key_f = split_heads(key_rows, DK)
    value_f = split_heads(value_rows, DV)
    log_cum = jnp.cumsum(split_heads(log_decay, DK), axis=2)
    log_last = log_cum[:, :, -1:, :]
    query_dec = query_f * jnp.exp(log_cum)
    key_dec = key_f * jnp.exp(-log_cum)
    causal = jnp.tril(jnp.ones((BLOCK, BLOCK), dtype=bool))
    scores = jnp.where(
        causal, jnp.einsum("hncd,hnsd->hncs", query_dec, key_dec, precision=highest), 0.0
    )
    inside = jnp.einsum("hncs,hnsv->hncv", scores, value_f, precision=highest)
    contrib = jnp.einsum(
        "hncd,hncv->hndv", key_f * jnp.exp(log_last - log_cum), value_f, precision=highest
    )
    decay_block = jnp.exp(log_last[:, :, 0, :])

    def advance(carry_state, inputs):
        decay_step, added = inputs
        return (decay_step[..., None] * carry_state + added, carry_state)

    start_state = jnp.zeros((head_count, DK, DV), jnp.float32)
    final_state, earlier = lax.scan(
        advance, start_state, (jnp.moveaxis(decay_block, 1, 0), jnp.moveaxis(contrib, 1, 0))
    )
    earlier = jnp.moveaxis(earlier, 0, 1)
    output = inside + jnp.einsum("hncd,hndv->hncv", query_dec, earlier, precision=highest)
    return output.transpose(1, 2, 0, 3).reshape(length, head_count, DV)


def body(
    tokens,
    attn_gain,
    w_query,
    w_key,
    w_value,
    w_low,
    w_lift,
    decay_bias,
    head_gain,
    w_out,
    ffn_gain,
    w_gate,
    w_up,
    w_down,
    final_gain,
):
    row_count = tokens.shape[0]
    whole_rows = gather_directly(tokens, "tp", 1)
    normed = rms_rows(whole_rows, attn_gain).astype(jnp.bfloat16)

    def add_pieces(source, pieces):
        return tuple(
            (
                jnp.dot(source, weight_piece, preferred_element_type=jnp.float32)
                for weight_piece in pieces
            )
        )

    query_sum, key_sum, value_sum = add_pieces(
        normed, side_by_side((w_query, w_key, w_value), "fs", 0, 1)
    )
    query_rows = query_sum.astype(jnp.bfloat16)
    key_rows = key_sum.astype(jnp.bfloat16)
    value_rows = value_sum.astype(jnp.bfloat16)
    low_rank = jnp.dot(normed, w_low, preferred_element_type=jnp.float32).astype(jnp.bfloat16)
    log_decay = (
        jax.nn.log_sigmoid(
            jnp.dot(low_rank, w_lift, preferred_element_type=jnp.float32) + decay_bias
        )
        / 16.0
    )
    head_count = query_rows.shape[1] // DK
    gla_out = blockwise_gla(query_rows, key_rows, value_rows, log_decay, head_count)
    mixed_heads = (
        rms_rows(gla_out, head_gain).reshape(row_count, head_count * DV).astype(jnp.bfloat16)
    )
    out_terms = jnp.dot(
        mixed_heads, gather_directly(w_out, "fs", 1), preferred_element_type=jnp.float32
    )
    own_sum = summed_on_arrival(out_terms.astype(jnp.bfloat16), "tp", 1)
    first_sum = (tokens.astype(jnp.float32) + own_sum).astype(jnp.bfloat16)
    full_rows = gather_directly(first_sum, "tp", 1)
    normed_ffn = rms_rows(full_rows, ffn_gain).astype(jnp.bfloat16)
    gate_rows, up_rows = add_pieces(normed_ffn, side_by_side((w_gate, w_up), "fs", 0, 1))
    hidden = (jax.nn.silu(gate_rows) * up_rows).astype(jnp.bfloat16)
    down_terms = jnp.dot(
        hidden, lax.all_gather(w_down, "fs", axis=1, tiled=True), preferred_element_type=jnp.float32
    )
    own_ffn = summed_on_arrival(down_terms.astype(jnp.bfloat16), "tp", 1)
    second_sum = first_sum.astype(jnp.float32) + own_ffn
    square_sum = over_copies(jnp.sum(second_sum * second_sum, axis=1), "tp")
    factor = lax.rsqrt(square_sum / D + epsilon)[:, None]
    return (second_sum * factor * final_gain).astype(jnp.bfloat16)


def solution(mesh):
    return jax.shard_map(
        body,
        mesh=mesh,
        in_specs=(
            P(("grp", "fs"), "tp"),
            P(),
            P("fs", "tp"),
            P("fs", "tp"),
            P("fs", "tp"),
            P(),
            P(None, "tp"),
            P("tp"),
            P(),
            P("tp", "fs"),
            P(),
            P("fs", "tp"),
            P("fs", "tp"),
            P("tp", "fs"),
            P("tp"),
        ),
        out_specs=P(("grp", "fs"), "tp"),
        check_vma=False,
    )
```

profile of v0, /device:TPU:33, one launch (start us, length us, event | category | flops | bytes accessed | tf_op | source)
XLA Modules:
  0.0 365.1 jit_solution(1852456690066622126)
XLA Ops:
  6.6 1.6 pad_maximum_fusion.1
  8.2 1.1 copy.65
  9.3 1.6 broadcast_in_dim.44
  10.8 24.1 %all-to-all-start = ((bf16[8,512,256]{1,2,0:T(8,128)(2,1)}), bf16[8,512,256]{1,2,0:T(8,128)(2,1)S(1)}, u32[]{:S(2)}, u32[]{:S(2)}) async-start(bf16[8,512,256]{1,2,0:T(8,128)(2,1)} %broadcast_in_dim.44), calls=%async_computation | async-start | bytes 4194304 | tf_op jit(solution)/shard_map/all_to_all | solution.py:18
  34.9 0.8 pad_maximum_fusion
  35.9 25.3 %all-to-all-done = bf16[8,512,256]{1,2,0:T(8,128)(2,1)S(1)} async-done(((bf16[8,512,256]{1,2,0:T(8,128)(2,1)}), bf16[8,512,256]{1,2,0:T(8,128)(2,1)S(1)}, u32[]{:S(2)}, u32[]{:S(2)}) %all-to-all-start) | async-done | bytes 2097184 | tf_op jit(solution)/shard_map/all_to_all | solution.py:18
  61.2 1.1 broadcast_in_dim.48
  62.3 5.8 %all-to-all-start.1 = ((bf16[16,256,128]{1,2,0:T(8,128)(2,1)}), bf16[16,256,128]{1,2,0:T(8,128)(2,1)S(1)}, u32[]{:S(2)}, u32[]{:S(2)}) async-start(bf16[16,256,128]{1,2,0:T(8,128)(2,1)} %broadcast_in_dim.48), calls=%async_computation.1 | async-start | bytes 2097152 | tf_op jit(solution)/shard_map/all_to_all | solution.py:18
  68.1 0.5 multiply_reduce_fusion.1
  68.6 1.9 fusion.4
  70.6 3.2 fusion.28
  73.8 1.1 fusion.36
  74.9 0.7 copy-done.5
  75.6 39.5 %all-gather.4.cloned.1.call-done = bf16[2048,512]{1,0:T(8,128)(2,1)} async-done(((bf16[128,512]{1,0:T(8,128)(2,1)}), bf16[2048,512]{1,0:T(8,128)(2,1)}) %all-gather.4.cloned.1.call-update) | async-done | bytes 2097168 | tf_op jit(solution)/shard_map/all_gather | solution.py:38
  115.2 1.9 convolution_convert_fusion.3
  117.2 0.7 fusion.17
  118.1 0.3 fusion.33
  118.4 0.8 convolution_convert_fusion.2
  119.2 0.6 convolution_bitcast_fusion
  119.8 0.6 convolution_select_fusion
  120.4 0.4 fusion.43
  120.8 6.2 %while.13 = (s32[]{:T(128)}, f32[1,128,256]{2,1,0:T(8,128)S(1)}, f32[8,1,128,256]{3,2,1,0:T(8,128)}, f32[8,1,128]{2,1,0:T(1,128)S(1)}, f32[8,1,128,256]{3,2,1,0:T(8,128)S(1)}, /*index=5*/s32[]{:T(128)}, s32[]{:T(128)}) while((s32[]{:T(128)}, f32[1,128,256]{2,1,0:T(8,128)S(1)}, f32[8,1,128,256]{3,2,1,0:T(8,128)}, ...), condition=%wide.region_3.4_spmd.clone, body=%wide.region_2.3_spmd.clone.sunk | while | flops 131075 | bytes 657504 | solution.py:96
  120.8 0.7 bitcast_dynamic-update-slice_fusion.2
  121.6 0.7 bitcast_dynamic-update-slice_fusion.2
  122.4 0.7 bitcast_dynamic-update-slice_fusion.2
  123.2 0.7 bitcast_dynamic-update-slice_fusion.2
  123.9 0.6 bitcast_dynamic-update-slice_fusion.2
  124.7 0.7 bitcast_dynamic-update-slice_fusion.2
  125.5 0.7 bitcast_dynamic-update-slice_fusion.2
  126.3 0.7 bitcast_dynamic-update-slice_fusion.2
  127.1 2.0 multiply_reduce_fusion.3
  129.2 0.8 convolution_convert_fusion
  130.0 1.5 copy.102
  131.5 16.1 %all-to-all-start.2 = ((bf16[8,512,256]{2,1,0:T(8,128)(2,1)}), bf16[8,512,256]{2,1,0:T(8,128)(2,1)S(1)}, u32[]{:S(2)}, u32[]{:S(2)}) async-start(bf16[8,512,256]{2,1,0:T(8,128)(2,1)} %bitcast.95), calls=%async_computation.2 | async-start | bytes 4194304 | tf_op jit(solution)/shard_map/all_to_all | solution.py:48
  147.6 0.7 all-gather.8.cloned.1.call-update
  148.3 25.4 %all-to-all-done.2 = bf16[8,512,256]{2,1,0:T(8,128)(2,1)S(1)} async-done(((bf16[8,512,256]{2,1,0:T(8,128)(2,1)}), bf16[8,512,256]{2,1,0:T(8,128)(2,1)S(1)}, u32[]{:S(2)}, u32[]{:S(2)}) %all-to-all-start.2) | async-done | bytes 2097184 | tf_op jit(solution)/shard_map/all_to_all | solution.py:48
  173.8 0.3 convert_reduce_fusion.1
  174.5 29.7 %all_to_all.31 = bf16[8,512,256]{1,2,0:T(8,128)(2,1)S(1)} all-to-all(bf16[8,512,256]{1,2,0:T(8,128)(2,1)S(1)} %broadcast_in_dim.49), channel_id=1, replica_groups=mesh['grp'=2,'fs'=16,'tp'=8] {'tp'}, dimensions={0} | all-to-all | bytes 4194304 | tf_op jit(solution)/shard_map/all_to_all | solution.py:18
  204.2 0.5 multiply_reduce_fusion
  204.8 0.5 fusion.2
  205.4 15.2 %all-gather.6.cloned.1.call-done = bf16[2048,1408]{0,1:T(8,128)(2,1)} async-done(((bf16[128,1408]{0,1:T(8,128)(2,1)}), bf16[2048,1408]{0,1:T(8,128)(2,1)}) %all-gather.6.cloned.1.call-update) | async-done | bytes 5767184 | tf_op jit(solution)/shard_map/all_gather | solution.py:38
  220.6 4.6 %fusion.7 = f32[512,704]{0,1:T(8,128)} fusion(bf16[512,2048]{0,1:T(8,128)(2,1)S(1)} %fusion.2, bf16[2048,1408]{0,1:T(8,128)(2,1)} %all-gather.6.cloned.1.call-done), kind=kOutput, calls=%fused_computation.18 | convolution fusion | flops 1476395008 | bytes 6422528 | tf_op jit(solution)/shard_map/dot_general | solution.py:128
  225.2 75.2 %all-gather.8.cloned.1.call-done = bf16[704,2048]{1,0:T(8,128)(2,1)} async-done(((bf16[704,128]{1,0:T(8,128)(2,1)}), bf16[704,2048]{1,0:T(8,128)(2,1)}) %all-gather.8.cloned.1.call-update) | async-done | bytes 2883600 | tf_op jit(solution)/shard_map/all_gather | solution.py:161
  300.3 7.1 %convolution_convert_fusion.1 = bf16[512,2048]{1,0:T(8,128)(2,1)S(1)} fusion(bf16[704,2048]{1,0:T(8,128)(2,1)} %all-gather.8.cloned.1.call-done, bf16[512,2048]{0,1:T(8,128)(2,1)} %copy-done.4, bf16[2048,1408]{0,1:T(8,128)(2,1)} %all-gather.6.cloned.1.call-done, f32[512,704]{0,1:T(8,128)} %fusion.7), kind=kOutput, calls=%fused_computation.15 | convolution fusion | flops 2956001280 | bytes 11403264 | tf_op jit(solution)/shard_map/dot_general | solution.py:160
  307.6 41.4 %all_to_all.32 = bf16[8,512,256]{2,1,0:T(8,128)(2,1)S(1)} all-to-all(bf16[8,512,256]{2,1,0:T(8,128)(2,1)S(1)} %bitcast.97), channel_id=1, replica_groups=mesh['grp'=2,'fs'=16,'tp'=8] {'tp'}, dimensions={0} | all-to-all | bytes 4194304 | tf_op jit(solution)/shard_map/all_to_all | solution.py:48
  349.1 0.3 convert_reduce_fusion
  349.5 8.1 %all_to_all.33 = f32[8,1,512]{2,1,0:T(1,128)S(1)} all-to-all(f32[8,1,512]{2,1,0:T(1,128)S(1)} %broadcast_in_dim.50), channel_id=1, replica_groups=mesh['grp'=2,'fs'=16,'tp'=8] {'tp'}, dimensions={0} | all-to-all | bytes 32768 | tf_op jit(solution)/shard_map/all_to_all | solution.py:18
  357.7 0.8 multiply_convert_fusion
  (75 shorter events, 2.2 us)
Async XLA Ops:
  6.5 64.0 %copy-start = (bf16[2048,32]{0,1:T(8,128)(2,1)S(1)}, bf16[2048,32]{0,1:T(8,128)(2,1)}, u32[]{:S(2)}) copy-start(bf16[2048,32]{0,1:T(8,128)(2,1)} %param.22) | copy-start | bytes 393220
  6.6 108.6 %all-gather.4.cloned.1.call-start = ((), (), s32[]{:S(2)}) async-start(), calls=%async_computation.6 | async-start | bytes 2228224 | tf_op jit(solution)/shard_map/all_gather | solution.py:38
  10.8 24.1 %copy-start.8 = (bf16[128,704]{0,1:T(8,128)(2,1)S(1)}, bf16[128,704]{0,1:T(8,128)(2,1)}, u32[]{:S(2)}) copy-start(bf16[128,704]{0,1:T(8,128)(2,1)} %param.29) | copy-start | bytes 540676
  10.8 24.1 %copy-start.9 = (bf16[128,704]{0,1:T(8,128)(2,1)S(1)}, bf16[128,704]{0,1:T(8,128)(2,1)}, u32[]{:S(2)}) copy-start(bf16[128,704]{0,1:T(8,128)(2,1)} %param.28) | copy-start | bytes 540676
  10.8 24.9 %copy-start.10 = (bf16[256,128]{1,0:T(8,128)(2,1)S(1)}, bf16[256,128]{1,0:T(8,128)(2,1)}, u32[]{:S(2)}) copy-start(bf16[256,128]{1,0:T(8,128)(2,1)} %param.26) | copy-start | bytes 196612
  10.8 50.4 %all-to-all-start = ((bf16[8,512,256]{1,2,0:T(8,128)(2,1)}), bf16[8,512,256]{1,2,0:T(8,128)(2,1)S(1)}, u32[]{:S(2)}, u32[]{:S(2)}) async-start(bf16[8,512,256]{1,2,0:T(8,128)(2,1)} %broadcast_in_dim.44), calls=%async_computation | async-start | bytes 4194304 | tf_op jit(solution)/shard_map/all_to_all | solution.py:18
  34.9 185.7 %all-gather.6.cloned.1.call-start = ((), (), s32[]{:S(2)}) async-start(), calls=%async_computation.7 | async-start | bytes 6127616 | tf_op jit(solution)/shard_map/all_gather | solution.py:38
  62.3 6.3 %copy-start.11 = (f32[2048]{0:T(1024)S(1)}, f32[2048]{0:T(1024)}, u32[]{:S(2)}) copy-start(f32[2048]{0:T(1024)} %param.18) | copy-start | bytes 24580
  62.3 66.9 %all-to-all-start.1 = ((bf16[16,256,128]{1,2,0:T(8,128)(2,1)}), bf16[16,256,128]{1,2,0:T(8,128)(2,1)S(1)}, u32[]{:S(2)}, u32[]{:S(2)}) async-start(bf16[16,256,128]{1,2,0:T(8,128)(2,1)} %broadcast_in_dim.48), calls=%async_computation.1 | async-start | bytes 2097152 | tf_op jit(solution)/shard_map/all_to_all | solution.py:18
  68.6 2.0 copy-start.12
  68.6 1.9 copy-start.16
  70.6 44.6 %copy-start.1 = (bf16[512,2048]{0,1:T(8,128)(2,1)S(1)}, bf16[512,2048]{0,1:T(8,128)(2,1)}, u32[]{:S(2)}) copy-start(bf16[512,2048]{0,1:T(8,128)(2,1)} %fusion.4) | copy-start | bytes 6291460
  74.9 0.7 copy-start.5
  115.2 2.0 copy-start.17
  117.1 1.0 copy-start.6
  118.4 1.4 copy-start.2
  120.4 6.6 %copy-start.3 = (f32[8,64,128]{2,0,1:T(8,128)S(1)}, f32[8,64,128]{2,0,1:T(8,128)}, u32[]{:S(2)}) copy-start(f32[8,64,128]{2,0,1:T(8,128)} %copy-done.2) | copy-start | bytes 786436
  120.8 8.4 %copy-start.15 = (f32[256]{0:T(256)S(1)}, f32[256]{0:T(256)}, u32[]{:S(2)}) copy-start(f32[256]{0:T(256)} %param.25) | copy-start | bytes 3076
  131.5 42.3 %all-to-all-start.2 = ((bf16[8,512,256]{2,1,0:T(8,128)(2,1)}), bf16[8,512,256]{2,1,0:T(8,128)(2,1)S(1)}, u32[]{:S(2)}, u32[]{:S(2)}) async-start(bf16[8,512,256]{2,1,0:T(8,128)(2,1)} %bitcast.95), calls=%async_computation.2 | async-start | bytes 4194304 | tf_op jit(solution)/shard_map/all_to_all | solution.py:48
  147.6 26.5 %copy-start.7 = (bf16[512,256]{1,0:T(8,128)(2,1)S(1)}, bf16[512,256]{1,0:T(8,128)(2,1)}, u32[]{:S(2)}) copy-start(bf16[512,256]{1,0:T(8,128)(2,1)} %param.17) | copy-start | bytes 786436
  147.6 152.7 %all-gather.8.cloned.1.call-start = ((), (), s32[]{:S(2)}) async-start(), calls=%async_computation.8 | async-start | bytes 3063808 | tf_op jit(solution)/shard_map/all_gather | solution.py:161
  204.1 0.7 copy-start.13
  205.4 19.8 %copy-start.4 = (bf16[512,2048]{0,1:T(8,128)(2,1)}, bf16[512,2048]{0,1:T(8,128)(2,1)S(1)}, u32[]{:S(2)}) copy-start(bf16[512,2048]{0,1:T(8,128)(2,1)S(1)} %fusion.2) | copy-start | bytes 6291460
  349.1 8.6 %copy-start.14 = (f32[256]{0:T(256)S(1)}, f32[256]{0:T(256)}, u32[]{:S(2)}) copy-start(f32[256]{0:T(256)} %param.31) | copy-start | bytes 3076
Sparse Core Ops, SparseCore 0:
  9.1 105.9 all-gather.3
  116.9 103.6 all-gather.5
  222.3 77.9 all-gather.7
where the time goes:
time: 366 us; the launch traced here: 365 us
  waiting for transfers between devices  181 us (49%)
  blocking collectives  79.2 us (22%)
  starting transfers between devices  46 us (13%)
  matrix products  22.7 us (6%)
  other arithmetic  15 us (4%)
  between operations  13.4 us (4%)
  local copies, waits for them, and re-layouts  7 us (2%)
    all_gather x1, waiting for transfers between devices, body(): lax.all_gather(w_down, 'fs', axis=1, tiled=True)  75.2 us
    all_gather x2, waiting for transfers between devices, side_by_side(): lax.all_gather(both, axis, axis=dim, tiled=True)  54.7 us
    all_to_all x1, blocking collectives, summed_on_arrival(): lax.all_to_all(blocks, axis, split_axis=0, concat_axis=0, tiled=True)  41.4 us
    all_to_all x2, blocking collectives, copy_for_each(): return lax.all_to_all(copies, axis, split_axis=0, concat_axis=0, tiled=True)  37.8 us
    all_to_all x2, starting transfers between devices, copy_for_each(): return lax.all_to_all(copies, axis, split_axis=0, concat_axis=0, tiled=True)  29.9 us
    all_to_all x1, waiting for transfers between devices, summed_on_arrival(): lax.all_to_all(blocks, axis, split_axis=0, concat_axis=0, tiled=True)  25.4 us
    all_to_all x2, waiting for transfers between devices, copy_for_each(): return lax.all_to_all(copies, axis, split_axis=0, concat_axis=0, tiled=True)  25.3 us
    all_to_all x1, starting transfers between devices, summed_on_arrival(): lax.all_to_all(blocks, axis, split_axis=0, concat_axis=0, tiled=True)  16.1 us
  transfers between devices with their start and end apart: 6, of which 5 were waited for; matrix products, arithmetic and copies ran while one was open for 9% of the time, Pallas kernels for 0%

commit v1 on v0

v1 whole, which is shorter than its diff:
```python
import functools

import jax
import jax.numpy as jnp
from jax import lax
from jax.experimental import pallas as pl
from jax.experimental.pallas import tpu as pltpu
from jax.sharding import PartitionSpec as P

DK = 128
DV = 256
BLOCK = 64
EPS = 1e-06
BF = jnp.bfloat16
F32 = jnp.float32
MESH = pl.DeviceIdType.MESH
HIGHEST = lax.Precision.HIGHEST


def dot(a, b, dims=((1,), (0,)), precision=None):
    return lax.dot_general(
        a, b, (dims, ((), ())), precision=precision, preferred_element_type=F32
    )


def kernel(
    n_fs, n_tp,
    tok, wq, wk, wv, wo, wg, wu, wt, wd, wl, ag, wlift, bias, hg, fg, fin,
    out,
    X, Gq, Go, Gg, Gd, N, QKV, C, M, F, H, SS, Q, state,
    PB1, D1, S1, B1, A1, PB2, D2, S2, B2, A2,
    lsem, zs, zr, ys, yr, xs, xr,
):
    rows, width = tok.shape
    d_model = width * n_tp
    half_rows = rows // 2
    half = n_fs // 2
    full = wt.shape[1] * 5 if False else (wg.shape[1] // 128) * 128
    units = wg.shape[1]
    kq, ko, kd = wq.shape[0], wo.shape[0], wd.shape[0]

    grp, z, me = lax.axis_index("grp"), lax.axis_index("fs"), lax.axis_index("tp")
    parity = lax.rem(grp, 2)
    partner = {"grp": grp + 1 - 2 * parity}
    z_up, z_down = {"fs": lax.rem(z + 1, n_fs)}, {"fs": lax.rem(z + n_fs - 1, n_fs)}
    core = lax.rem(me, 2)

    def at_tp(offset):
        return lax.rem(me + offset + n_tp, n_tp)

    def other(slot):
        return slot + 1 - 2 * core

    r_slot, l_slot, o_slot = at_tp(2), at_tp(-2), at_tp(4)
    right, left, sib = {"tp": r_slot}, {"tp": l_slot}, {"tp": other(me)}
    sends = []

    def remote(src, dst, ssem, rsem, device):
        return pltpu.make_async_remote_copy(
            src_ref=src, dst_ref=dst, send_sem=ssem, recv_sem=rsem,
            device_id=device, device_id_type=MESH,
        )

    def send(src, dst, ssem, rsem, device):
        copy = remote(src, dst, ssem, rsem, device)
        copy.start()
        sends.append((src, dst, ssem, rsem, device))

    def arrived(ref, ssem, rsem):
        remote(ref, ref, ssem, rsem, sib).wait_recv()

    zq = pl.multiple_of(z * kq, kq)
    local = [
        (tok, X.at[me]),
        (wq, Gq.at[pl.ds(zq, kq), pl.ds(0, DK)]),
        (wk, Gq.at[pl.ds(zq, kq), pl.ds(DK, DK)]),
        (wv, Gq.at[pl.ds(zq, kq), pl.ds(2 * DK, DV)]),
        (wg.at[:, pl.ds(0, full)], Gg.at[pl.ds(zq, kq), pl.ds(0, full)]),
        (wu.at[:, pl.ds(0, full)], Gg.at[pl.ds(zq, kq), pl.ds(full, full)]),
        (wt, Gg.at[pl.ds(zq, kq), pl.ds(2 * full, 128)]),
        (wo, Go.at[z]),
        (wd, Gd.at[z, pl.ds(0, kd), :]),
    ]
    local = [pltpu.make_async_copy(s, d, lsem.at[i]) for i, (s, d) in enumerate(local)]
    for copy in local:
        copy.start()

    barrier = pltpu.get_barrier_semaphore()
    greeted = [z_up, z_down, partner] + [{"tp": at_tp(k)} for k in range(1, n_tp)]
    for device in greeted:
        pl.semaphore_signal(barrier, inc=1, device_id=device, device_id_type=MESH)
    if kd < Gd.shape[1]:
        Gd[:, kd:, :] = jnp.zeros((n_fs, Gd.shape[1] - kd, 128), BF)
        H[:, units:] = jnp.zeros((rows, H.shape[1] - units), BF)
    pl.semaphore_wait(barrier, len(greeted))

    def by_rows(view, base, total, edge):
        chunk, other_edge = total - edge, total - edge

        def part(shard, start, size):
            return view(shard, pl.multiple_of(base + start, 16), size)

        first = (chunk // 2 + 15) // 16 * 16
        return dict(
            ring=lambda s: part(s, parity * edge, chunk),
            mine=lambda s: part(s, parity * other_edge, edge),
            theirs=lambda s: part(s, (1 - parity) * other_edge, edge),
            halves=(
                lambda s: part(s, parity * edge, first),
                lambda s: part(s, parity * edge + first, chunk - first),
            ),
        )

    def gate_up(base, size):
        total = Gg.shape[1]
        edge = (total // 128 * 3 // 8) * 128
        chunk = total - edge

        def part(shard, r0, rn, start, cols):
            row = pl.multiple_of(shard * kq + base + r0, 16)
            return Gg.at[pl.ds(row, rn), pl.ds(pl.multiple_of(start, 128), cols)]

        return dict(
            ring=lambda s: part(s, 0, size, parity * edge, chunk),
            mine=lambda s: part(s, 0, size, parity * chunk, edge),
            theirs=lambda s: part(s, 0, size, (1 - parity) * chunk, edge),
            halves=(
                lambda s: part(s, 0, size // 2, parity * edge, chunk),
                lambda s: part(s, size // 2, size // 2, parity * edge, chunk),
            ),
        )

    def view_q(shard, start, size):
        return Gq.at[pl.ds(pl.multiple_of(shard * kq + start, 16), size), :]

    streams = [
        by_rows(view_q, 0, kq, 48),
        by_rows(lambda s, start, size: Go.at[s, pl.ds(start, size), :], 0, ko, 80),
    ]
    streams += [gate_up(k * 32, 32) for k in range(kq // 32)]
    half_d = kd // 2
    streams += [
        by_rows(lambda s, start, size: Gd.at[s, pl.ds(start, size), :], k * half_d, half_d, 96)
        for k in range(2)
    ]
    QS, OS, G0, G1, G2, G3, E0, E1 = range(8)

    def launch(i):
        ref = streams[i]["ring"](z)
        send(ref, ref, zs.at[i, 0, 0], zr.at[i, 0, 0], z_up)
        send(ref, ref, zs.at[i, 1, 0], zr.at[i, 1, 0], z_down)

    def event(i, s):
        st = streams[i]
        for way, (shard, device) in enumerate(
            ((lax.rem(z - s + n_fs, n_fs), z_up), (lax.rem(z + s, n_fs), z_down))
        ):
            if s < half:
                arrived(st["ring"](shard), zs.at[i, way, s - 1], zr.at[i, way, s - 1])
                ref = st["ring"](shard) if s + 1 < half else st["halves"][way](shard)
                send(ref, ref, zs.at[i, way, s], zr.at[i, way, s], device)
            else:
                ref = st["halves"][way](shard)
                arrived(ref, zs.at[i, way, s - 1], zr.at[i, way, s - 1])
            if s < half or way == 1:
                ref = st["mine"](shard)
                send(ref, ref, ys.at[i, way, s - 1], yr.at[i, way, s - 1], partner)

    def imported(i):
        for s in range(1, half + 1):
            for way, shard in enumerate((lax.rem(z - s + n_fs, n_fs), lax.rem(z + s, n_fs))):
                if s < half or way == 1:
                    ref = streams[i]["theirs"](shard)
                    arrived(ref, ys.at[i, way, s - 1], yr.at[i, way, s - 1])

    queue = []

    def serve(count):
        for _ in range(min(count, len(queue))):
            item = queue.pop(0)
            if item[1] == 0:
                launch(item[0])
            else:
                event(*item)

    top, low = pl.ds(0, half_rows), pl.ds(half_rows, half_rows)

    def gather_stages(buf, base):
        def go(k, slot, part, device):
            ref = buf.at[slot] if part is None else buf.at[slot, part, :]
            send(ref, ref, xs.at[base + k], xr.at[base + k], device)

        def got(k, slot, part):
            ref = buf.at[slot] if part is None else buf.at[slot, part, :]
            arrived(ref, xs.at[base + k], xr.at[base + k])

        def s0():
            go(0, me, top, right)
            go(2, me, low, left)
            go(1, me, low, right)
            go(3, me, top, left)
            go(4, me, None, sib)

        def s1():
            got(0, l_slot, top)
            go(5, l_slot, top, right)
            go(6, l_slot, top, sib)
            got(2, r_slot, low)
            go(7, r_slot, low, left)
            go(8, r_slot, low, sib)

        def s2():
            got(1, l_slot, low)
            go(9, l_slot, low, sib)
            got(3, r_slot, top)
            go(10, r_slot, top, sib)

        def s3():
            got(5, o_slot, top)
            go(11, o_slot, top, sib)
            got(7, o_slot, low)
            go(12, o_slot, low, sib)

        def s4():
            got(4, other(me), None)
            got(6, other(l_slot), top)
            got(8, other(r_slot), low)
            got(9, other(l_slot), low)
            got(10, other(r_slot), top)
            got(11, other(o_slot), top)
            got(12, other(o_slot), low)

        return s0, s1, s2, s3, s4

    def scatter_stages(PB, D, S, B, A, base):
        def go(k, src, dst, device):
            send(src, dst, xs.at[base + k], xr.at[base + k], device)

        def got(k, dst):
            arrived(dst, xs.at[base + k], xr.at[base + k])

        def add(dst, start, count, terms):
            step = 64

            @pl.loop(0, count // step)
            def _(t):
                r = pl.ds(pl.multiple_of(start + t * step, step), step)
                total = terms[0](r).astype(F32)
                for term in terms[1:]:
                    total = total + term(r).astype(F32)
                dst[r, :] = total.astype(BF)

        def s0():
            for k, slot in enumerate((o_slot, r_slot, l_slot, me)):
                go(k, PB.at[other(slot)], D.at[k], sib)

        def s1():
            got(0, D.at[0])
            add(S.at[0], 0, rows, [lambda r: PB[o_slot, r, :], lambda r: D[0, r, :]])
            go(4, S.at[0, top, :], A.at[0], right)
            go(5, S.at[0, low, :], A.at[1], left)
            got(1, D.at[1])
            add(S.at[1], half_rows, half_rows, [lambda r: PB[r_slot, r, :], lambda r: D[1, r, :]])
            go(6, S.at[1, low, :], B.at[0, low, :], right)
            got(2, D.at[2])
            add(S.at[2], 0, half_rows, [lambda r: PB[l_slot, r, :], lambda r: D[2, r, :]])
            go(7, S.at[2, top, :], B.at[1, top, :], left)

        def s2():
            got(4, A.at[0])
            add(S.at[1], 0, half_rows,
                [lambda r: PB[r_slot, r, :], lambda r: D[1, r, :], lambda r: A[0, r, :]])
            go(8, S.at[1, top, :], B.at[0, top, :], right)
            got(5, A.at[1])

            @pl.loop(0, half_rows // 64)
            def _(t):
                ra = pl.ds(pl.multiple_of(t * 64, 64), 64)
                r = pl.ds(pl.multiple_of(half_rows + t * 64, 64), 64)
                total = PB[l_slot, r, :].astype(F32) + D[2, r, :].astype(F32) + A[1, ra, :].astype(F32)
                S[2, r, :] = total.astype(BF)

            go(9, S.at[2, low, :], B.at[1, low, :], left)

        def s3():
            got(3, D.at[3])
            got(6, B.at[0, low, :])
            got(7, B.at[1, top, :])
            got(8, B.at[0, top, :])
            got(9, B.at[1, low, :])

        def own(r):
            return (
                PB[me, r, :].astype(F32) + D[3, r, :].astype(F32)
                + B[0, r, :].astype(F32) + B[1, r, :].astype(F32)
            )

        return s0, s1, s2, s3, own

    def normalize(buf, gain):
        step = 32

        @pl.loop(0, rows // step)
        def _(t):
            r = pl.ds(pl.multiple_of(t * step, step), step)
            blocks = [buf[j, r, :].astype(F32) for j in range(n_tp)]
            squares = blocks[0] * blocks[0]
            for b in blocks[1:]:
                squares = squares + b * b
            factor = lax.rsqrt(jnp.sum(squares, axis=1, keepdims=True) * (1.0 / d_model) + EPS)
            for j, b in enumerate(blocks):
                cols = pl.ds(j * width, width)
                N[r, cols] = (b * factor * gain[:, cols]).astype(BF)

    ti = lax.broadcasted_iota(jnp.int32, (BLOCK, BLOCK), 0)
    si = lax.broadcasted_iota(jnp.int32, (BLOCK, BLOCK), 1)

    def decay():
        tril = jnp.where(ti >= si, 1.0, 0.0).astype(BF)
        step = 2 * BLOCK

        @pl.loop(0, rows // step)
        def _(t):
            r = pl.ds(pl.multiple_of(t * step, step), step)
            rank = dot(N[r, :], wl[...]).astype(BF)
            v = dot(rank, wlift[...]) + bias[...]
            log_decay = (jnp.minimum(v, 0.0) - jnp.log1p(jnp.exp(-jnp.abs(v)))) * (1.0 / 16.0)
            for k in range(2):
                part = log_decay[k * BLOCK : (k + 1) * BLOCK]
                hi = part.astype(BF)
                lo = (part - hi.astype(F32)).astype(BF)
                r2 = pl.ds(pl.multiple_of(t * step + k * BLOCK, BLOCK), BLOCK)
                C[r2, :] = dot(tril, hi) + dot(tril, lo)

    def project(t):
        step = rows // 4
        r = pl.ds(t * step, step)
        QKV[r, :] = dot(N[r, :], Gq[...]).astype(BF)

    def attend(t):
        r = pl.ds(t * BLOCK, BLOCK)
        c = C[r, :]
        last = C[pl.ds((t + 1) * BLOCK - 1, 1), :]
        q = QKV[r, pl.ds(0, DK)].astype(F32) * DK ** (-0.5)
        k = QKV[r, pl.ds(DK, DK)].astype(F32)
        v = QKV[r, pl.ds(2 * DK, DV)]
        q_dec = (q * jnp.exp(c)).astype(BF)
        k_dec = (k * jnp.exp(-c)).astype(BF)
        k_end = (k * jnp.exp(last - c)).astype(BF)
        scores = jnp.where(ti >= si, dot(q_dec, k_dec, ((1,), (1,))), 0.0).astype(BF)
        o = dot(scores, v)
        if t > 0:
            o = o + dot(q_dec, state[...].astype(BF), ((1,), (1,)))
        added = dot(v, k_end, ((0,), (0,)))
        state[...] = state[...] * jnp.exp(last) + added if t > 0 else added
        factor = lax.rsqrt(jnp.mean(o * o, axis=1, keepdims=True) + EPS)
        M[r, :] = (o * factor * hg[...]).astype(BF)

    def partial_products(left_ref, G, PB):
        step = rows // 2

        @pl.loop(0, n_tp)
        def _(j):
            weight = jnp.concatenate([G[2 * j], G[2 * j + 1]], axis=1)
            for t in range(2):
                r = pl.ds(t * step, step)
                PB[j, r, :] = dot(left_ref[r, :], weight).astype(BF)

    def feed(t, at, size):
        step = rows // 2
        r = pl.ds(t * step, step)
        if at < full:
            gate = dot(N[r, :], Gg[:, pl.ds(at, size)])
            up = dot(N[r, :], Gg[:, pl.ds(full + at, size)])
        else:
            both = dot(N[r, :], Gg[:, pl.ds(2 * full, 2 * size)])
            gate, up = both[:, :size], both[:, size:]
        H[r, pl.ds(at, size)] = (gate / (1.0 + jnp.exp(-gate)) * up).astype(BF)

    queue += [(QS, 0), (OS, 0), (G0, 0)]
    for s in range(1, half + 1):
        queue += [(QS, s), (OS, s), (G0, s)]
        if s >= half - 1:
            queue += [(G1, 0), (G2, 0)] if s == half - 1 else [(G3, 0), (E0, 0), (E1, 0)]
    for s in range(1, half + 1):
        queue += [(G1, s), (G2, s), (G3, s), (E0, s), (E1, s)]

    g0, g1, g2, g3, g4 = gather_stages(X, 0)
    local[0].wait()
    g0()
    for copy in local[1:4]:
        copy.wait()
    serve(1)
    for copy in local[4:]:
        copy.wait()
    serve(2)
    serve(3)
    g1()
    serve(3)
    g2()
    serve(3)
    g3()
    serve(3)
    g4()
    normalize(X, ag)
    serve(3)
    decay()
    serve(100 if False else 3 * (half - 5) + 5)
    serve(3)
    imported(QS)
    for t in range(4):
        project(t)
        serve(1)
    for t in range(rows // BLOCK):
        attend(t)
        serve(1)
    imported(OS)
    partial_products(M, Go, PB1)
    s0, s1, s2, s3, own = scatter_stages(PB1, D1, S1, B1, A1, 13)
    s0()
    serve(2)
    s1()
    serve(4)
    s2()
    serve(4)
    s3()

    @pl.loop(0, rows // 64)
    def _(t):
        r = pl.ds(pl.multiple_of(t * 64, 64), 64)
        F[me, r, :] = (X[me, r, :].astype(F32) + own(r)).astype(BF)

    g0, g1, g2, g3, g4 = gather_stages(F, 23)
    g0()
    serve(4)
    g1()
    serve(2)
    g2()
    serve(2)
    g3()
    serve(1)
    g4()
    normalize(F, fg)
    serve(len(queue))
    for i in (G0, G1, G2, G3):
        imported(i)
    for t in range(2):
        for at in range(0, full, 256):
            feed(t, at, min(256, full - at))
        feed(t, full, units - full)
    for i in (E0, E1):
        imported(i)
    partial_products(H, Gd, PB2)
    s0, s1, s2, s3, own = scatter_stages(PB2, D2, S2, B2, A2, 36)
    s0()
    s1()
    s2()
    s3()

    @pl.loop(0, rows // 64)
    def _(t):
        r = pl.ds(pl.multiple_of(t * 64, 64), 64)
        SS[r, :] = F[me, r, :].astype(F32) + own(r)

    second = SS[...]
    Q[me] = dot(jnp.ones((8, width), F32), second * second, ((1,), (1,)), HIGHEST)
    for k in range(1, n_tp):
        send(Q.at[me], Q.at[me], xs.at[46 + k], xr.at[46 + k], {"tp": at_tp(k)})
    for k in range(1, n_tp):
        arrived(Q.at[at_tp(-k)], xs.at[46 + k], xr.at[46 + k])
    squares = Q[0]
    for j in range(1, n_tp):
        squares = squares + Q[j]
    factor = lax.rsqrt(squares * (1.0 / d_model) + EPS)
    factor = dot(factor, jnp.full((8, width), 0.125, F32), ((0,), (0,)), HIGHEST)
    out[...] = (SS[...] * factor * fin[...]).astype(BF)

    for item in sends:
        remote(*item).wait_send()


def body(n_fs, n_tp, tokens, attn_gain, w_query, w_key, w_value, w_low, w_lift, decay_bias, head_gain,
         w_out, ffn_gain, w_gate, w_up, w_down, final_gain):
    rows, width = tokens.shape
    d_model = width * n_tp
    units = w_gate.shape[1]
    full = units // 128 * 128
    kq, ko, kd = w_query.shape[0], w_out.shape[0], w_down.shape[0]
    kd_pad = (kd + 127) // 128 * 128
    tails = jnp.concatenate([w_gate[:, full:], w_up[:, full:]], axis=1)
    any_space = pl.BlockSpec(memory_space=pl.ANY)
    vmem = pl.BlockSpec(memory_space=pltpu.VMEM)

    def scratch(*shape, dtype=BF):
        return pltpu.VMEM(shape, dtype)

    def exchange():
        return [
            scratch(n_tp, rows, width), scratch(4, rows, width), scratch(3, rows, width),
            scratch(2, rows, width), scratch(2, rows // 2, width),
        ]

    half = n_fs // 2
    n_streams = 4 + kq // 32
    ring = pltpu.SemaphoreType.DMA((n_streams, 2, half))
    return pl.pallas_call(
        functools.partial(kernel, n_fs, n_tp),
        out_shape=jax.ShapeDtypeStruct((rows, width), BF),
        in_specs=[any_space] * 9 + [vmem] * 7,
        out_specs=vmem,
        scratch_shapes=[
            scratch(n_tp, rows, width),
            scratch(d_model, 2 * DK + DV),
            scratch(n_fs, ko, 128),
            scratch(d_model, 2 * units),
            scratch(n_fs, kd_pad, 128),
            scratch(rows, d_model),
            scratch(rows, 2 * DK + DV),
            scratch(rows, DK, dtype=F32),
            scratch(rows, DV),
            scratch(n_tp, rows, width),
            scratch(rows, kd_pad),
            scratch(rows, width, dtype=F32),
            scratch(n_tp, 8, rows, dtype=F32),
            scratch(DV, DK, dtype=F32),
            *exchange(),
            *exchange(),
            pltpu.SemaphoreType.DMA((9,)),
            ring, ring, ring, ring,
            pltpu.SemaphoreType.DMA((54,)),
            pltpu.SemaphoreType.DMA((54,)),
        ],
        compiler_params=pltpu.CompilerParams(
            collective_id=0, has_side_effects=True, vmem_limit_bytes=60 * 1024 * 1024
        ),
    )(
        tokens, w_query, w_key, w_value, w_out, w_gate, w_up, tails, w_down,
        w_low, attn_gain.reshape(1, -1), w_lift, decay_bias.reshape(1, -1), head_gain.reshape(1, -1),
        ffn_gain.reshape(1, -1), final_gain.reshape(1, -1),
    )


def solution(mesh):
    n_fs, n_tp = mesh.shape["fs"], mesh.shape["tp"]
    if mesh.shape["grp"] % 2 or n_tp != 8:
        raise ValueError("unsupported mesh")
    return jax.shard_map(
        functools.partial(body, n_fs, n_tp),
        mesh=mesh,
        in_specs=(
            P(("grp", "fs"), "tp"),
            P(),
            P("fs", "tp"),
            P("fs", "tp"),
            P("fs", "tp"),
            P(),
            P(None, "tp"),
            P("tp"),
            P(),
            P("tp", "fs"),
            P(),
            P("fs", "tp"),
            P("fs", "tp"),
            P("tp", "fs"),
            P("tp"),
        ),
        out_specs=P(("grp", "fs"), "tp"),
        check_vma=False,
    )
```

time: 366 us -> 154 us (0.42)
  waiting for transfers between devices: 181 us -> 0 us
  Pallas kernels: 0 us -> 148 us
  blocking collectives: 79.2 us -> 0 us
  starting transfers between devices: 46 us -> 0 us
  matrix products: 22.7 us -> 0 us
  other arithmetic: 15 us -> 0.68 us
  between operations: 13.4 us -> 0.05 us
    pallas_call x0 -> x1, Pallas kernels: none -> 148 us  [body(): pl.pallas_call(functools.partial(kernel, n_fs, n_tp), out_shape=jax.Shape...]
    all_gather x3 -> x0, waiting for transfers between devices: 130 us -> none  [the longest x1 75.2 us: body(): lax.all_gather(w_down, 'fs', axis=1, tiled=True)]
    all_to_all x3 -> x0, blocking collectives: 79.2 us -> none  [the longest x1 41.4 us: summed_on_arrival(): lax.all_to_all(blocks, axis, split_axis=0, concat_axis=0, tiled=True)]
    all_to_all x3 -> x0, waiting for transfers between devices: 50.7 us -> none  [the longest x1 25.4 us: summed_on_arrival(): lax.all_to_all(blocks, axis, split_axis=0, concat_axis=0, tiled=True)]
    all_to_all x3 -> x0, starting transfers between devices: 46 us -> none  [the longest x2 29.9 us: copy_for_each(): return lax.all_to_all(copies, axis, split_axis=0, concat_axis=0, tiled=True)]
    dot_general x11 -> x0, matrix products: 22.7 us -> none  [the longest x4 8.01 us: add_pieces(): jnp.dot(source, weight_piece, preferred_element_type=jnp.float32)]
    dynamic_update_slice x8 -> x0, other arithmetic: 5.25 us -> none  [blockwise_gla(): lax.scan(advance, start_state, (jnp.moveaxis(decay_block, 1, 0), jnp.move...]
  transfers between devices with their start and end apart: 6 -> 0, of which waited for: 5 -> 0; matrix products, arithmetic and copies ran while one was open for 9% -> 0% of each run, Pallas kernels for 0% -> 0%
where the time goes in v1:
time: 154 us
  Pallas kernels  148 us (96%)
  local copies, waits for them, and re-layouts  4.72 us (3%)
    pallas_call x1, Pallas kernels, body(): pl.pallas_call(functools.partial(kernel, n_fs, n_tp), out_shape=jax.Shape...  148 us
    unnamed x12, local copies, waits for them, and re-layouts  4.71 us

profile of v1, /device:TPU:33, one launch (start us, length us, event | category | flops | bytes accessed | tf_op | source)
XLA Modules:
  0.0 153.6 jit_solution(12440433033107698300)
XLA Ops:
  0.0 0.0 copy-start.2
  0.0 1.1 copy.18.wg
  1.1 0.0 copy-start
  1.1 0.0 copy-done.2
  1.1 0.1 copy.19.wu
  1.3 0.5 copy-done
  1.8 0.0 copy-start.1
  1.8 0.0 copy-start.3
  1.8 0.7 pad_maximum_fusion.wt
  2.5 0.3 copy-done.3
  2.8 1.0 copy.20.wl
  3.8 0.0 copy-done.1
  3.8 148.1 %shard_map.145 = bf16[512,256]{1,0:T(8,128)(2,1)} custom-call(bf16[512,256]{1,0:T(8,128)(2,1)} %tok.1, bf16[128,128]{1,0:T(8,128)(2,1)} %wq.1, bf16[128,128]{1,0:T(8,128)(2,1)} %wk.1, bf16[128,256]{1,0:T(8,128)(2,1)} %wv.1, bf16[256,128]{1,0:T(8,128)(2,1)} %wo.1, bf16[128,704]{1,0:T(8,128)(2,1)} %copy-done, bf16[128,704]{1,0:T(8,128)(2,1)} %copy-done.1, ...), custom_call_target="tpu_custom_call" | custom-call | tf_op jit(solution)/shard_map/pallas_call | solution.py:506
  151.9 1.7 %copy.22 = bf16[512,256]{1,0:T(8,128)(2,1)} copy(bf16[512,256]{1,0:T(8,128)(2,1)} %shard_map.145) | data formatting | bytes 524288
  (2 shorter events, 0.0 us)
Async XLA Ops:
  0.0 1.1 copy-start.2
  1.1 0.7 copy-start
  1.8 2.0 %copy-start.1 = (bf16[128,704]{1,0:T(8,128)(2,1)}, bf16[128,704]{1,0:T(8,128)(2,1)S(1)}, u32[]{:S(2)}) copy-start(bf16[128,704]{1,0:T(8,128)(2,1)S(1)} %copy.19.wu) | copy-start | bytes 540676
  1.8 1.0 copy-start.3

commit v2 on v1

v2 whole, which is shorter than its diff:
```python
import functools

import jax
import jax.numpy as jnp
from jax import lax
from jax.experimental import pallas as pl
from jax.experimental.pallas import tpu as pltpu
from jax.sharding import PartitionSpec as P

DK = 128
DV = 256
BLOCK = 64
EPS = 1e-06
BF = jnp.bfloat16
F32 = jnp.float32
MESH = pl.DeviceIdType.MESH
HIGHEST = lax.Precision.HIGHEST


def dot(a, b, dims=((1,), (0,)), precision=None):
    return lax.dot_general(
        a, b, (dims, ((), ())), precision=precision, preferred_element_type=F32
    )


def kernel(
    n_fs, n_tp,
    tok, wq, wk, wv, wo, wg, wu, wd, wl, ag, wlift, bias, hg, fg,
    out,
    X, Gq, Go, Gg, Gd, N, QKV, C, M, F, H, SS, Q, state,
    PB1, D1, S1, B1, A1, T1, PB2, D2, S2, B2, A2, T2,
    lsem, zs, zr, ys, yr, xs, xr,
):
    rows, width = tok.shape
    d_model = width * n_tp
    half_rows = rows // 2
    half = n_fs // 2
    units = wg.shape[0]
    kq, ko, kd = wq.shape[0], wo.shape[0], wd.shape[0]

    grp, z, me = lax.axis_index("grp"), lax.axis_index("fs"), lax.axis_index("tp")
    parity = lax.rem(grp, 2)
    partner = {"grp": grp + 1 - 2 * parity}
    z_up, z_down = {"fs": lax.rem(z + 1, n_fs)}, {"fs": lax.rem(z + n_fs - 1, n_fs)}
    core = lax.rem(me, 2)

    def at_tp(offset):
        return lax.rem(me + offset + n_tp, n_tp)

    def other(slot):
        return slot + 1 - 2 * core

    r_slot, l_slot, o_slot = at_tp(2), at_tp(-2), at_tp(4)
    right, left, sib = {"tp": r_slot}, {"tp": l_slot}, {"tp": other(me)}

    def remote(src, dst, ssem, rsem, device):
        return pltpu.make_async_remote_copy(
            src_ref=src, dst_ref=dst, send_sem=ssem, recv_sem=rsem,
            device_id=device, device_id_type=MESH,
        )

    def send(src, dst, ssem, rsem, device):
        remote(src, dst, ssem, rsem, device).start()

    def arrived(ref, rsem):
        remote(ref, ref, xs.at[0], rsem, sib).wait_recv()

    def sent(ref, ssem):
        remote(ref, ref, ssem, xr.at[0], sib).wait_send()

    zq = pl.multiple_of(z * kq, kq)
    local = [
        (tok, X.at[me]),
        (wq, Gq.at[pl.ds(zq, kq), pl.ds(0, DK)]),
        (wk, Gq.at[pl.ds(zq, kq), pl.ds(DK, DK)]),
        (wv, Gq.at[pl.ds(zq, kq), pl.ds(2 * DK, DV)]),
        (wo, Go.at[z]),
        (wg, Gg.at[z, pl.ds(0, units), :]),
        (wu, Gg.at[z, pl.ds(units, units), :]),
        (wd, Gd.at[z, pl.ds(0, kd), :]),
    ]
    local = [pltpu.make_async_copy(s, d, lsem.at[i]) for i, (s, d) in enumerate(local)]
    for copy in local:
        copy.start()

    barrier = pltpu.get_barrier_semaphore()
    greeted = [z_up, z_down, partner] + [{"tp": at_tp(k)} for k in range(1, n_tp)]
    for device in greeted:
        pl.semaphore_signal(barrier, inc=1, device_id=device, device_id_type=MESH)
    if kd < Gd.shape[1]:
        Gd[:, kd:, :] = jnp.zeros((n_fs, Gd.shape[1] - kd, 128), BF)
        H[:, units:] = jnp.zeros((rows, H.shape[1] - units), BF)
    pl.semaphore_wait(barrier, len(greeted))

    def by_rows(view, base, total, edge):
        chunk, other_edge = total - edge, total - edge

        def part(shard, start, size):
            return view(shard, pl.multiple_of(base + start, 16), size)

        first = (chunk // 2 + 15) // 16 * 16
        return dict(
            ring=lambda s: part(s, parity * edge, chunk),
            mine=lambda s: part(s, parity * other_edge, edge),
            theirs=lambda s: part(s, (1 - parity) * other_edge, edge),
            sizes=(chunk, edge),
            halves=(
                lambda s: part(s, parity * edge, first),
                lambda s: part(s, parity * edge + first, chunk - first),
            ),
        )

    def view_q(shard, start, size):
        return Gq.at[pl.ds(pl.multiple_of(shard * kq + start, 16), size), :]

    def view_of(G):
        return lambda shard, start, size: G.at[shard, pl.ds(start, size), :]

    half_q, half_d = kq // 2, kd // 2
    streams = [
        by_rows(view_q, 0, half_q, 16),
        by_rows(view_q, half_q, half_q, 32),
        by_rows(view_of(Go), 0, ko, 80),
    ]
    streams += [by_rows(view_of(Gg), k * half_d, half_d, 112 if k % 2 == 0 else 96) for k in range(4)]
    streams += [by_rows(view_of(Gd), k * half_d, half_d, 96) for k in range(2)]
    QA, QB, OS, G0, G1, U0, U1, E0, E1 = range(9)

    def launch(i):
        ref = streams[i]["ring"](z)
        send(ref, ref, zs.at[i], zr.at[i, 0, 0], z_up)
        send(ref, ref, zs.at[i], zr.at[i, 1, 0], z_down)

    def event(i, s):
        st = streams[i]
        for way, (shard, device) in enumerate(
            ((lax.rem(z - s + n_fs, n_fs), z_up), (lax.rem(z + s, n_fs), z_down))
        ):
            if s < half:
                arrived(st["ring"](shard), zr.at[i, way, s - 1])
                ref = st["ring"](shard) if s + 1 < half else st["halves"][way](shard)
                send(ref, ref, zs.at[i], zr.at[i, way, s], device)
            else:
                arrived(st["halves"][way](shard), zr.at[i, way, s - 1])
            if s < half or way == 1:
                ref = st["mine"](shard)
                send(ref, ref, ys.at[i], yr.at[i], partner)

    def others(size):
        return Gg.at[pl.ds(0, n_fs - 1), pl.ds(0, size), :]

    def lanes(i):
        return 4 if i in (QA, QB) else 1

    def imported(i):
        arrived(others(streams[i]["sizes"][1] * lanes(i)), yr.at[i])

    queue = []

    def serve(count):
        while queue and (count or queue[0][1] == 0):
            item = queue.pop(0)
            if item[1] == 0:
                launch(item[0])
            else:
                event(*item)
                count -= 1

    def serve_to(*item):
        serve(sum(step > 0 for _, step in queue[: queue.index(item) + 1]))

    top, low = pl.ds(0, half_rows), pl.ds(half_rows, half_rows)

    def gather_stages(buf, base, family):
        def go(k, slot, part, device):
            ref = buf.at[slot] if part is None else buf.at[slot, part, :]
            send(ref, ref, xs.at[family], xr.at[base + k], device)

        def got(k, slot, part):
            ref = buf.at[slot] if part is None else buf.at[slot, part, :]
            arrived(ref, xr.at[base + k])

        def s0():
            go(0, me, top, right)
            go(2, me, low, left)
            go(1, me, low, right)
            go(3, me, top, left)
            go(4, me, None, sib)

        def s1():
            got(0, l_slot, top)
            go(5, l_slot, top, right)
            go(6, l_slot, top, sib)
            got(2, r_slot, low)
            go(7, r_slot, low, left)
            go(8, r_slot, low, sib)

        def s2():
            got(1, l_slot, low)
            go(9, l_slot, low, sib)
            got(3, r_slot, top)
            go(10, r_slot, top, sib)

        def s3():
            got(5, o_slot, top)
            go(11, o_slot, top, sib)
            got(7, o_slot, low)
            go(12, o_slot, low, sib)

        def s4():
            got(4, other(me), None)
            got(6, other(l_slot), top)
            got(8, other(r_slot), low)
            got(9, other(l_slot), low)
            got(10, other(r_slot), top)
            got(11, other(o_slot), top)
            got(12, other(o_slot), low)

        return s0, s1, s2, s3, s4

    def scatter_stages(left_ref, G, PB, D, S, B, A, T, SS, base, family):
        def go(k, src, dst, device):
            send(src, dst, xs.at[family], xr.at[base + k], device)

        def got(k, dst):
            arrived(dst, xr.at[base + k])

        def product(slot, part):
            weight = jnp.concatenate([G[2 * slot], G[2 * slot + 1]], axis=1)
            return dot(left_ref[part, :], weight)

        def s0(k):
            slot = other((o_slot, r_slot, l_slot, me)[k])
            for part in (top, low):
                PB[k, part, :] = product(slot, part).astype(BF)
            go(k, PB.at[k], D.at[k], sib)

        def s1(k):
            slot = (o_slot, r_slot, l_slot, me)[k]
            parts = [product(slot, part) for part in (top, low)]
            got(k, D.at[k])
            parts = [p + D[k, part, :].astype(F32) for p, part in zip(parts, (top, low))]
            if k == 0:
                S[0, top, :] = parts[0].astype(BF)
                go(4, S.at[0, top, :], A.at[0], right)
                S[0, low, :] = parts[1].astype(BF)
                go(5, S.at[0, low, :], A.at[1], left)
            elif k == 1:
                S[1, low, :] = parts[1].astype(BF)
                go(6, S.at[1, low, :], B.at[0, low, :], right)
                T[0] = parts[0]
            elif k == 2:
                S[2, top, :] = parts[0].astype(BF)
                go(7, S.at[2, top, :], B.at[1, top, :], left)
                T[1] = parts[1]
            else:
                SS[top, :] = parts[0]
                SS[low, :] = parts[1]

        def s2():
            got(4, A.at[0])
            S[1, top, :] = (T[0] + A[0].astype(F32)).astype(BF)
            go(8, S.at[1, top, :], B.at[0, top, :], right)
            got(5, A.at[1])
            S[2, low, :] = (T[1] + A[1].astype(F32)).astype(BF)
            go(9, S.at[2, low, :], B.at[1, low, :], left)

        def s3():
            got(6, B.at[0, low, :])
            got(7, B.at[1, top, :])
            got(8, B.at[0, top, :])
            got(9, B.at[1, low, :])

        def own(r):
            return SS[r, :] + B[0, r, :].astype(F32) + B[1, r, :].astype(F32)

        return s0, s1, s2, s3, own

    def normalize(buf, gain):
        step = 32

        @pl.loop(0, rows // step)
        def _(t):
            r = pl.ds(pl.multiple_of(t * step, step), step)
            blocks = [buf[j, r, :].astype(F32) for j in range(n_tp)]
            squares = blocks[0] * blocks[0]
            for b in blocks[1:]:
                squares = squares + b * b
            factor = lax.rsqrt(jnp.sum(squares, axis=1, keepdims=True) * (1.0 / d_model) + EPS)
            for j, b in enumerate(blocks):
                cols = pl.ds(j * width, width)
                N[r, cols] = (b * factor * gain[:, cols]).astype(BF)

    ti = lax.broadcasted_iota(jnp.int32, (BLOCK, BLOCK), 0)
    si = lax.broadcasted_iota(jnp.int32, (BLOCK, BLOCK), 1)

    def decay(part):
        tril = jnp.where(ti >= si, 1.0, 0.0).astype(BF)
        step = 2 * BLOCK

        @pl.loop(part * (rows // step // 2), (part + 1) * (rows // step // 2))
        def _(t):
            r = pl.ds(pl.multiple_of(t * step, step), step)
            rank = dot(N[r, :], wl[...], ((1,), (1,))).astype(BF)
            v = dot(rank, wlift[...]) + bias[...]
            log_decay = (jnp.minimum(v, 0.0) - jnp.log1p(jnp.exp(-jnp.abs(v)))) * (1.0 / 16.0)
            for k in range(2):
                part = log_decay[k * BLOCK : (k + 1) * BLOCK]
                hi = part.astype(BF)
                lo = (part - hi.astype(F32)).astype(BF)
                r2 = pl.ds(pl.multiple_of(t * step + k * BLOCK, BLOCK), BLOCK)
                C[r2, :] = dot(tril, hi) + dot(tril, lo)

    def project(t):
        step = rows // 4
        r = pl.ds(t * step, step)
        QKV[r, :] = dot(N[r, :], Gq[...]).astype(BF)

    def attend(t):
        r = pl.ds(t * BLOCK, BLOCK)
        c = C[r, :]
        last = C[pl.ds((t + 1) * BLOCK - 1, 1), :]
        q = QKV[r, pl.ds(0, DK)].astype(F32) * DK ** (-0.5)
        k = QKV[r, pl.ds(DK, DK)].astype(F32)
        v = QKV[r, pl.ds(2 * DK, DV)]
        q_dec = (q * jnp.exp(c)).astype(BF)
        k_dec = (k * jnp.exp(-c)).astype(BF)
        k_end = (k * jnp.exp(last - c)).astype(BF)
        scores = jnp.where(ti >= si, dot(q_dec, k_dec, ((1,), (1,))), 0.0).astype(BF)
        o = dot(scores, v)
        if t > 0:
            o = o + dot(q_dec, state[...].astype(BF), ((1,), (1,)))
        added = dot(v, k_end, ((0,), (0,)))
        state[...] = state[...] * jnp.exp(last) + added if t > 0 else added
        factor = lax.rsqrt(jnp.mean(o * o, axis=1, keepdims=True) + EPS)
        M[r, :] = (o * factor * hg[...]).astype(BF)

    def feed(t, at, size):
        step = rows // 2
        r = pl.ds(t * step, step)

        def product(start):
            weight = jnp.concatenate([Gg[j, pl.ds(start, size), :] for j in range(n_fs)], axis=1)
            return dot(N[r, :], weight, ((1,), (1,)))

        gate, up = product(at), product(units + at)
        H[r, pl.ds(at, size)] = (gate / (1.0 + jnp.exp(-gate)) * up).astype(BF)

    queue += [(QA, 0), (QB, 0), (OS, 0), (G0, 0)]
    for s in range(1, half + 1):
        queue += [(QA, s), (QB, s), (OS, s), (G0, s)]
        if s == half - 1:
            queue += [(U0, 0), (G1, 0)]
        if s == half:
            queue += [(U1, 0)]
    for s in range(1, half + 1):
        queue += [(U0, s), (G1, s), (U1, s)]
        if s == 1:
            queue += [(E0, 0), (E1, 0)]
        if s > 1:
            queue += [(E0, s - 1), (E1, s - 1)]
    queue += [(E0, half), (E1, half)]

    g0, g1, g2, g3, g4 = gather_stages(X, 0, 0)
    local[0].wait()
    g0()
    for copy in local[1:]:
        copy.wait()
    serve_to(OS, 1)
    g1()
    serve_to(OS, 2)
    g2()
    serve_to(OS, 3)
    g3()
    serve_to(OS, 4)
    g4()
    normalize(X, ag)
    serve_to(OS, 5)
    decay(0)
    serve_to(OS, 6)
    decay(1)
    serve_to(OS, half)
    serve(2)
    imported(QA)
    imported(QB)
    for t in range(4):
        project(t)
        if t % 2:
            serve(1)
    for t in range(rows // BLOCK):
        attend(t)
        if t in (2, 5):
            serve(1)
    imported(OS)
    s0, s1, s2, s3, own = scatter_stages(M, Go, PB1, D1, S1, B1, A1, T1, SS, 13, 1)
    for k in range(4):
        s0(k)
    serve(1)
    for k in range(4):
        s1(k)
    serve(5)
    s2()
    serve(5)
    s3()

    @pl.loop(0, rows // 64)
    def _(t):
        r = pl.ds(pl.multiple_of(t * 64, 64), 64)
        F[me, r, :] = (X[me, r, :].astype(F32) + own(r)).astype(BF)

    g0, g1, g2, g3, g4 = gather_stages(F, 23, 2)
    g0()
    serve(6)
    g1()
    serve(3)
    g2()
    serve(2)
    g3()
    serve(1)
    g4()
    normalize(F, fg)
    serve_to(U1, half)
    for i in (G0, U0, G1, U1):
        imported(i)
    for t in range(2):
        for at in range(0, units, 256):
            feed(t, at, min(256, units - at))
            serve(1)
    serve(1000)
    for i in (E0, E1):
        imported(i)
    s0, s1, s2, s3, own = scatter_stages(H, Gd, PB2, D2, S2, B2, A2, T2, SS, 36, 3)
    for k in range(4):
        s0(k)
    for k in range(4):
        s1(k)
    s2()
    s3()

    ones = jnp.ones((8, width), BF)

    def in_two(v):
        hi = v.astype(BF)
        return hi, (v - hi.astype(F32)).astype(BF)

    with jax.named_scope("second"):
        for part in (top, low):
            second = F[me, part, :].astype(F32) + own(part)
            SS[part, :] = second
            Q[me, :, part] = sum(dot(ones, v, ((1,), (1,))) for v in in_two(second * second))
    with jax.named_scope("squares"):
        for k in range(1, n_tp):
            send(Q.at[me], Q.at[me], xs.at[4], xr.at[46 + k], {"tp": at_tp(k)})
        for k in range(1, n_tp):
            arrived(Q.at[at_tp(-k)], xr.at[46 + k])
    with jax.named_scope("close"):
        squares = Q[0]
        for j in range(1, n_tp):
            squares = squares + Q[j]
        eighth = jnp.full((8, width), 0.125, BF)
        factors = in_two(lax.rsqrt(squares * (1.0 / d_model) + EPS))
        for part in (0, half_rows):
            factor = sum(dot(v[:, part : part + half_rows], eighth, ((0,), (0,))) for v in factors)
            out[pl.ds(part, half_rows), :] = SS[pl.ds(part, half_rows), :] * factor
    with jax.named_scope("drain"):
        for i, st in enumerate(streams):
            sent(others(st["sizes"][0] * lanes(i)), zs.at[i])
            sent(others(st["sizes"][1] * lanes(i)), ys.at[i])
        for family in range(4):
            sent(X.at[pl.ds(0, n_tp - 1)], xs.at[family])
        sent(Q.at[pl.ds(0, n_tp - 1)], xs.at[4])


def body(n_fs, n_tp, tokens, attn_gain, w_query, w_key, w_value, w_low, w_lift, decay_bias, head_gain,
         w_out, ffn_gain, w_gate, w_up, w_down, final_gain):
    rows, width = tokens.shape
    d_model = width * n_tp
    units = w_gate.shape[1]
    kq, ko, kd = w_query.shape[0], w_out.shape[0], w_down.shape[0]
    kd_pad = (kd + 127) // 128 * 128
    any_space = pl.BlockSpec(memory_space=pl.ANY)
    vmem = pl.BlockSpec(memory_space=pltpu.VMEM)

    def scratch(*shape, dtype=BF):
        return pltpu.VMEM(shape, dtype)

    def exchange():
        return [
            scratch(4, rows, width), scratch(4, rows, width), scratch(3, rows, width),
            scratch(2, rows, width), scratch(2, rows // 2, width), scratch(2, rows // 2, width, dtype=F32),
        ]

    half = n_fs // 2
    n_streams = 9
    ring = pltpu.SemaphoreType.DMA((n_streams, 2, half))
    per_stream = pltpu.SemaphoreType.DMA((n_streams,))
    result = pl.pallas_call(
        functools.partial(kernel, n_fs, n_tp),
        out_shape=jax.ShapeDtypeStruct((rows, width), F32),
        in_specs=[any_space] * 8 + [vmem] * 6,
        out_specs=vmem,
        scratch_shapes=[
            scratch(n_tp, rows, width),
            scratch(d_model, 2 * DK + DV),
            scratch(n_fs, ko, 128),
            scratch(n_fs, 2 * units, 128),
            scratch(n_fs, kd_pad, 128),
            scratch(rows, d_model),
            scratch(rows, 2 * DK + DV),
            scratch(rows, DK, dtype=F32),
            scratch(rows, DV),
            scratch(n_tp, rows, width),
            scratch(rows, kd_pad),
            scratch(rows, width, dtype=F32),
            scratch(n_tp, 8, rows, dtype=F32),
            scratch(DV, DK, dtype=F32),
            *exchange(),
            *exchange(),
            pltpu.SemaphoreType.DMA((8,)),
            per_stream, ring, per_stream, per_stream,
            pltpu.SemaphoreType.DMA((5,)),
            pltpu.SemaphoreType.DMA((54,)),
        ],
        compiler_params=pltpu.CompilerParams(
            collective_id=0, has_side_effects=True, vmem_limit_bytes=67043328
        ),
    )(
        tokens, w_query, w_key, w_value, w_out, w_gate.T, w_up.T, w_down,
        w_low.T, attn_gain.reshape(1, -1), w_lift, decay_bias.reshape(1, -1), head_gain.reshape(1, -1),
        ffn_gain.reshape(1, -1),
    )
    return (result * final_gain).astype(BF)


def solution(mesh):
    n_fs, n_tp = mesh.shape["fs"], mesh.shape["tp"]
    if mesh.shape["grp"] % 2 or n_tp != 8:
        raise ValueError("unsupported mesh")
    return jax.shard_map(
        functools.partial(body, n_fs, n_tp),
        mesh=mesh,
        in_specs=(
            P(("grp", "fs"), "tp"),
            P(),
            P("fs", "tp"),
            P("fs", "tp"),
            P("fs", "tp"),
            P(),
            P(None, "tp"),
            P("tp"),
            P(),
            P("tp", "fs"),
            P(),
            P("fs", "tp"),
            P("fs", "tp"),
            P("tp", "fs"),
            P("tp"),
        ),
        out_specs=P(("grp", "fs"), "tp"),
        check_vma=False,
    )
```

time: 154 us -> 142 us (0.922)
  Pallas kernels: 148 us -> 140 us
  local copies, waits for them, and re-layouts: 4.72 us -> 0 us
    pallas_call x1, Pallas kernels: 148 us -> 140 us  [body(): pl.pallas_call(functools.partial(kernel, n_fs, n_tp), out_shape=jax.Shape...]
    unnamed x12 -> x0, local copies, waits for them, and re-layouts: 4.71 us -> none
    convert_element_type x0 -> x1, other arithmetic: none -> 1.79 us  [body(): return (result * final_gain).astype(BF)]
where the time goes in v2:
time: 142 us
  Pallas kernels  140 us (99%)
  other arithmetic  1.79 us (1%)
    pallas_call x1, Pallas kernels, body(): pl.pallas_call(functools.partial(kernel, n_fs, n_tp), out_shape=jax.Shape...  140 us

profile of v2, /device:TPU:33, one launch (start us, length us, event | category | flops | bytes accessed | tf_op | source)
XLA Modules:
  0.0 142.1 jit_solution(884671980081752380)
XLA Ops:
  0.0 140.3 %shard_map.145 = f32[512,256]{1,0:T(8,128)} custom-call(bf16[512,256]{1,0:T(8,128)(2,1)} %tok.1, bf16[128,128]{1,0:T(8,128)(2,1)} %wq.1, bf16[128,128]{1,0:T(8,128)(2,1)} %wk.1, bf16[128,256]{1,0:T(8,128)(2,1)} %wv.1, bf16[256,128]{1,0:T(8,128)(2,1)} %wo.1, bf16[704,128]{1,0:T(8,128)(2,1)} %bitcast.7, bf16[704,128]{1,0:T(8,128)(2,1)} %bitcast.8, ...), custom_call_target="tpu_custom_call" | custom-call | tf_op jit(solution)/shard_map/pallas_call | solution.py:497
  140.3 1.8 %multiply_convert_fusion = bf16[512,256]{1,0:T(8,128)(2,1)} fusion(f32[512,256]{1,0:T(8,128)} %shard_map.145, f32[256]{0:T(256)} %param.29), kind=kLoop, calls=%fused_computation | loop fusion | flops 262144 | bytes 787456 | tf_op jit(solution)/shard_map/convert_element_type | solution.py:532

commit v3 on v2

--- a/solution.py
+++ b/solution.py
@@ -11,6 +11,7 @@
 DV = 256
 BLOCK = 64
 EPS = 1e-06
+START, LATENCY, RATE = 2.3, 2.6, 46.6e3
 BF = jnp.bfloat16
 F32 = jnp.float32
 MESH = pl.DeviceIdType.MESH
@@ -25,8 +26,9 @@
 
 def kernel(
     n_fs, n_tp,
-    tok, wq, wk, wv, wo, wg, wu, wd, wl, ag, wlift, bias, hg, fg,
+    tok, wq, wk, wv, wo, wg, wu, wd, wl_in, ag_in, wlift_in, bias_in, hg_in, fg_in, fin_in,
     out,
+    wl, ag, wlift, bias, hg, fg, fin,
     X, Gq, Go, Gg, Gd, N, QKV, C, M, F, H, SS, Q, state,
     PB1, D1, S1, B1, A1, T1, PB2, D2, S2, B2, A2, T2,
     lsem, zs, zr, ys, yr, xs, xr,
@@ -68,6 +70,10 @@
     def sent(ref, ssem):
         remote(ref, ref, ssem, xr.at[0], sib).wait_send()
 
+    barrier = pltpu.get_barrier_semaphore()
+    greeted = [z_up, z_down, partner] + [{"tp": at_tp(k)} for k in range(1, n_tp)]
+    for device in greeted:
+        pl.semaphore_signal(barrier, inc=1, device_id=device, device_id_type=MESH)
     zq = pl.multiple_of(z * kq, kq)
     local = [
         (tok, X.at[me]),
@@ -83,10 +89,11 @@
     for copy in local:
         copy.start()
 
-    barrier = pltpu.get_barrier_semaphore()
-    greeted = [z_up, z_down, partner] + [{"tp": at_tp(k)} for k in range(1, n_tp)]
-    for device in greeted:
-        pl.semaphore_signal(barrier, inc=1, device_id=device, device_id_type=MESH)
+    small = [(wl_in, wl), (ag_in, ag), (wlift_in, wlift), (bias_in, bias), (hg_in, hg), (fg_in, fg), (fin_in, fin)]
+    small = [pltpu.make_async_copy(s, d, lsem.at[8 + i]) for i, (s, d) in enumerate(small)]
+    for copy in small:
+        copy.start()
+
     if kd < Gd.shape[1]:
         Gd[:, kd:, :] = jnp.zeros((n_fs, Gd.shape[1] - kd, 128), BF)
         H[:, units:] = jnp.zeros((rows, H.shape[1] - units), BF)
@@ -116,58 +123,85 @@
     def view_of(G):
         return lambda shard, start, size: G.at[shard, pl.ds(start, size), :]
 
-    half_q, half_d = kq // 2, kd // 2
+    half_q, half_d, tail = kq // 2, kd // 2, units - 2 * 256
     streams = [
         by_rows(view_q, 0, half_q, 16),
         by_rows(view_q, half_q, half_q, 32),
         by_rows(view_of(Go), 0, ko, 80),
+        by_rows(view_of(Gg), 0, 256, 80),
+        by_rows(view_of(Gg), units, 256, 80),
+        by_rows(view_of(Gg), 256, 256, 80),
+        by_rows(view_of(Gg), units + 256, 256, 80),
+        by_rows(view_of(Gg), 512, tail, 80),
+        by_rows(view_of(Gg), units + 512, tail, 80),
+        by_rows(view_of(Gd), 0, half_d, 96),
+        by_rows(view_of(Gd), half_d, half_d, 96),
     ]
-    streams += [by_rows(view_of(Gg), k * half_d, half_d, 112 if k % 2 == 0 else 96) for k in range(4)]
-    streams += [by_rows(view_of(Gd), k * half_d, half_d, 96) for k in range(2)]
-    QA, QB, OS, G0, G1, U0, U1, E0, E1 = range(9)
+    QA, QB, OS, G0, U0, G1, U1, G2, U2, E0, E1 = range(11)
 
     def launch(i):
         ref = streams[i]["ring"](z)
-        send(ref, ref, zs.at[i], zr.at[i, 0, 0], z_up)
-        send(ref, ref, zs.at[i], zr.at[i, 1, 0], z_down)
+        send(ref, ref, zs.at[i], zr.at[i, 0], z_up)
+        send(ref, ref, zs.at[i], zr.at[i, 0], z_down)
 
     def event(i, s):
         st = streams[i]
-        for way, (shard, device) in enumerate(
-            ((lax.rem(z - s + n_fs, n_fs), z_up), (lax.rem(z + s, n_fs), z_down))
-        ):
+        flows = ((lax.rem(z - s + n_fs, n_fs), z_up), (lax.rem(z + s, n_fs), z_down))
+        arrived(some(1 if s == half else 2, st["sizes"][0] * lanes(i)), zr.at[i, s - 1])
+        for way, (shard, device) in enumerate(flows):
             if s < half:
-                arrived(st["ring"](shard), zr.at[i, way, s - 1])
                 ref = st["ring"](shard) if s + 1 < half else st["halves"][way](shard)
-                send(ref, ref, zs.at[i], zr.at[i, way, s], device)
-            else:
-                arrived(st["halves"][way](shard), zr.at[i, way, s - 1])
+                send(ref, ref, zs.at[i], zr.at[i, s], device)
+        for way, (shard, device) in enumerate(flows):
             if s < half or way == 1:
                 ref = st["mine"](shard)
                 send(ref, ref, ys.at[i], yr.at[i], partner)
 
+    def some(shards, size):
+        return Gg.at[pl.ds(0, shards), pl.ds(0, size), :]
+
     def others(size):
-        return Gg.at[pl.ds(0, n_fs - 1), pl.ds(0, size), :]
+        return some(n_fs - 1, size)
 
     def lanes(i):
         return 4 if i in (QA, QB) else 1
 
-    def imported(i):
-        arrived(others(streams[i]["sizes"][1] * lanes(i)), yr.at[i])
+    def imported(*which):
+        for i in which:
+            arrived(others(streams[i]["sizes"][1] * lanes(i)), yr.at[i])
 
     queue = []
 
-    def serve(count):
-        while queue and (count or queue[0][1] == 0):
-            item = queue.pop(0)
-            if item[1] == 0:
-                launch(item[0])
-            else:
-                event(*item)
-                count -= 1
-
-    def serve_to(*item):
-        serve(sum(step > 0 for _, step in queue[: queue.index(item) + 1]))
+    left_at, clock, link = {}, [START], [START]
+
+    def due(until=None):
+        until = clock[0] if until is None else until
+        while queue:
+            i, s = queue[0]
+            arrival = left_at[i, s - 1] + LATENCY if s else clock[0]
+            if arrival > until:
+                break
+            queue.pop(0)
+            with jax.named_scope("ev%d_%d" % (i, s)):
+                if s == 0:
+                    launch(i)
+                else:
+                    event(i, s)
+            clock[0] = max(clock[0], arrival) + (0.1 if s else 0.0)
+            if s < half:
+                weight = streams[i]["sizes"][0] * lanes(i) * 256 / RATE
+                link[0] = max(link[0], clock[0]) + weight * (0.5 if s == half - 1 else 1)
+                left_at[i, s] = link[0]
+        clock[0] = max(clock[0], min(until, 1000.0))
+
+    def due_to(*item):
+        while item in queue:
+            i, s = queue[0]
+            due(left_at[i, s - 1] + LATENCY if s else clock[0])
+
+    def work(us):
+        clock[0] += us
+        due()
 
     top, low = pl.ds(0, half_rows), pl.ds(half_rows, half_rows)
 
@@ -229,6 +263,9 @@
             weight = jnp.concatenate([G[2 * slot], G[2 * slot + 1]], axis=1)
             return dot(left_ref[part, :], weight)
 
+        def quarter(q):
+            return pl.ds(q * (half_rows // 2), half_rows // 2)
+
         def s0(k):
             slot = other((o_slot, r_slot, l_slot, me)[k])
             for part in (top, low):
@@ -241,10 +278,12 @@
             got(k, D.at[k])
             parts = [p + D[k, part, :].astype(F32) for p, part in zip(parts, (top, low))]
             if k == 0:
-                S[0, top, :] = parts[0].astype(BF)
-                go(4, S.at[0, top, :], A.at[0], right)
-                S[0, low, :] = parts[1].astype(BF)
-                go(5, S.at[0, low, :], A.at[1], left)
+                for way in range(2):
+                    S[0, (top, low)[way], :] = parts[way].astype(BF)
+                for h in range(2):
+                    for way in range(2):
+                        src = S.at[0, quarter(2 * way + h), :]
+                        go((4, 10, 5, 11)[2 * way + h], src, A.at[way, quarter(h), :], (right, left)[way])
             elif k == 1:
                 S[1, low, :] = parts[1].astype(BF)
                 go(6, S.at[1, low, :], B.at[0, low, :], right)
@@ -257,29 +296,28 @@
                 SS[top, :] = parts[0]
                 SS[low, :] = parts[1]
 
-        def s2():
-            got(4, A.at[0])
-            S[1, top, :] = (T[0] + A[0].astype(F32)).astype(BF)
-            go(8, S.at[1, top, :], B.at[0, top, :], right)
-            got(5, A.at[1])
-            S[2, low, :] = (T[1] + A[1].astype(F32)).astype(BF)
-            go(9, S.at[2, low, :], B.at[1, low, :], left)
+        def s2(h):
+            for way in range(2):
+                q = quarter(2 * way + h)
+                got((4, 10, 5, 11)[2 * way + h], A.at[way, quarter(h), :])
+                S[1 + way, q, :] = (T[way, quarter(h), :] + A[way, quarter(h), :].astype(F32)).astype(BF)
+                go((8, 12, 9, 13)[2 * way + h], S.at[1 + way, q, :], B.at[way, q, :], (right, left)[way])
 
         def s3():
             got(6, B.at[0, low, :])
             got(7, B.at[1, top, :])
-            got(8, B.at[0, top, :])
-            got(9, B.at[1, low, :])
+            for k, way, q in ((8, 0, 0), (9, 1, 2), (12, 0, 1), (13, 1, 3)):
+                got(k, B.at[way, quarter(q), :])
 
         def own(r):
             return SS[r, :] + B[0, r, :].astype(F32) + B[1, r, :].astype(F32)
 
         return s0, s1, s2, s3, own
 
-    def normalize(buf, gain):
+    def normalize(buf, gain, part):
         step = 32
 
-        @pl.loop(0, rows // step)
+        @pl.loop(part * (rows // step // 4), (part + 1) * (rows // step // 4))
         def _(t):
             r = pl.ds(pl.multiple_of(t * step, step), step)
             blocks = [buf[j, r, :].astype(F32) for j in range(n_tp)]
@@ -298,7 +336,7 @@
         tril = jnp.where(ti >= si, 1.0, 0.0).astype(BF)
         step = 2 * BLOCK
 
-        @pl.loop(part * (rows // step // 2), (part + 1) * (rows // step // 2))
+        @pl.loop(part * (rows // step // 4), (part + 1) * (rows // step // 4))
         def _(t):
             r = pl.ds(pl.multiple_of(t * step, step), step)
             rank = dot(N[r, :], wl[...], ((1,), (1,))).astype(BF)
@@ -346,122 +384,126 @@
         gate, up = product(at), product(units + at)
         H[r, pl.ds(at, size)] = (gate / (1.0 + jnp.exp(-gate)) * up).astype(BF)
 
-    queue += [(QA, 0), (QB, 0), (OS, 0), (G0, 0)]
-    for s in range(1, half + 1):
-        queue += [(QA, s), (QB, s), (OS, s), (G0, s)]
-        if s == half - 1:
-            queue += [(U0, 0), (G1, 0)]
-        if s == half:
-            queue += [(U1, 0)]
-    for s in range(1, half + 1):
-        queue += [(U0, s), (G1, s), (U1, s)]
-        if s == 1:
-            queue += [(E0, 0), (E1, 0)]
-        if s > 1:
-            queue += [(E0, s - 1), (E1, s - 1)]
-    queue += [(E0, half), (E1, half)]
-
-    g0, g1, g2, g3, g4 = gather_stages(X, 0, 0)
+    plan = (((QA, QB, OS, G0), 0), ((U0, G1, U1), 6), ((G2, U2), 7), ((E0, E1), 8))
+    for r in range(half + 9):
+        for group, start in plan:
+            if 0 <= r - start <= half:
+                queue += [(i, r - start) for i in group]
+
+    def gather(buf, base, family):
+        g0, g1, g2, g3, g4 = gather_stages(buf, base, family)
+        g0()
+        begun = clock[0]
+        for stage, ready in ((g1, 5.1), (g2, 7.8), (g3, 10.3), (g4, 11.1)):
+            due(begun + ready - 0.2)
+            stage()
+            work(0.1)
+
+    def scatter(stages):
+        s0, s1, s2, s3, own = stages
+        for k in range(3):
+            s0(k)
+            work(0.25)
+        begun = clock[0] + 0.3
+        s1(0)
+        s0(3)
+        work(0.6)
+        for k in range(1, 4):
+            s1(k)
+            work(0.27)
+        due(begun + 4.2)
+        s2(0)
+        work(0.1)
+        due(begun + 5.4)
+        s2(1)
+        work(0.1)
+        due(begun + 10.0)
+        s3()
+        return own
+
     local[0].wait()
-    g0()
     for copy in local[1:]:
         copy.wait()
-    serve_to(OS, 1)
-    g1()
-    serve_to(OS, 2)
-    g2()
-    serve_to(OS, 3)
-    g3()
-    serve_to(OS, 4)
-    g4()
-    normalize(X, ag)
-    serve_to(OS, 5)
-    decay(0)
-    serve_to(OS, 6)
-    decay(1)
-    serve_to(OS, half)
-    serve(2)
-    imported(QA)
-    imported(QB)
+    due()
+    gather(X, 0, 0)
+    for copy in small:
+        copy.wait()
+    for t in range(4):
+        normalize(X, ag, t)
+        work(0.55)
+    for t in range(4):
+        decay(t)
+        work(0.6)
+    due_to(QB, half)
+    due(clock[0] + 3.0)
+    imported(QA, QB)
     for t in range(4):
         project(t)
-        if t % 2:
-            serve(1)
+        work(0.37)
     for t in range(rows // BLOCK):
         attend(t)
-        if t in (2, 5):
-            serve(1)
+        work(0.2)
     imported(OS)
-    s0, s1, s2, s3, own = scatter_stages(M, Go, PB1, D1, S1, B1, A1, T1, SS, 13, 1)
-    for k in range(4):
-        s0(k)
-    serve(1)
-    for k in range(4):
-        s1(k)
-    serve(5)
-    s2()
-    serve(5)
-    s3()
+    own = scatter(scatter_stages(M, Go, PB1, D1, S1, B1, A1, T1, SS, 13, 1))
 
     @pl.loop(0, rows // 64)
     def _(t):
         r = pl.ds(pl.multiple_of(t * 64, 64), 64)
         F[me, r, :] = (X[me, r, :].astype(F32) + own(r)).astype(BF)
 
-    g0, g1, g2, g3, g4 = gather_stages(F, 23, 2)
-    g0()
-    serve(6)
-    g1()
-    serve(3)
-    g2()
-    serve(2)
-    g3()
-    serve(1)
-    g4()
-    normalize(F, fg)
-    serve_to(U1, half)
-    for i in (G0, U0, G1, U1):
-        imported(i)
+    work(0.3)
+    gather(F, 27, 2)
+    for t in range(4):
+        normalize(F, fg, t)
+        work(0.55)
+    due_to(E1, half - 2)
+    imported(G0, U0, G1, U1)
+    feed(0, 0, 256)
+    feed(0, 256, 256)
+    feed(1, 0, 256)
+    clock[0] += 2.3
+    due_to(E1, half - 1)
+    feed(1, 256, 256)
+    imported(G2, U2)
     for t in range(2):
-        for at in range(0, units, 256):
-            feed(t, at, min(256, units - at))
-            serve(1)
-    serve(1000)
-    for i in (E0, E1):
-        imported(i)
-    s0, s1, s2, s3, own = scatter_stages(H, Gd, PB2, D2, S2, B2, A2, T2, SS, 36, 3)
-    for k in range(4):
-        s0(k)
-    for k in range(4):
-        s1(k)
-    s2()
-    s3()
+        feed(t, 512, units - 512)
+    clock[0] += 2.3
+    due(10000.0)
+    imported(E0, E1)
+    own = scatter(scatter_stages(H, Gd, PB2, D2, S2, B2, A2, T2, SS, 40, 3))
 
     ones = jnp.ones((8, width), BF)
+    row = lax.broadcasted_iota(jnp.int32, (8, 128), 0)
 
     def in_two(v):
         hi = v.astype(BF)
         return hi, (v - hi.astype(F32)).astype(BF)
 
     with jax.named_scope("second"):
-        for part in (top, low):
+        packed = jnp.zeros((8, 128), F32)
+        for b in range(rows // 128):
+            part = pl.ds(b * 128, 128)
             second = F[me, part, :].astype(F32) + own(part)
             SS[part, :] = second
-            Q[me, :, part] = sum(dot(ones, v, ((1,), (1,))) for v in in_two(second * second))
+            sums = sum(dot(ones, v, ((1,), (1,))) for v in in_two(second * second))
+            packed = jnp.where(row == b, sums, packed)
+        Q[me] = packed
     with jax.named_scope("squares"):
+        for k in (4, 5, 3, 2, 6, 7, 1):
+            send(Q.at[me], Q.at[me], xs.at[4], xr.at[53 + k], {"tp": at_tp(k)})
         for k in range(1, n_tp):
-            send(Q.at[me], Q.at[me], xs.at[4], xr.at[46 + k], {"tp": at_tp(k)})
-        for k in range(1, n_tp):
-            arrived(Q.at[at_tp(-k)], xr.at[46 + k])
+            arrived(Q.at[at_tp(-k)], xr.at[53 + k])
     with jax.named_scope("close"):
         squares = Q[0]
         for j in range(1, n_tp):
             squares = squares + Q[j]
-        eighth = jnp.full((8, width), 0.125, BF)
-        factors = in_two(lax.rsqrt(squares * (1.0 / d_model) + EPS))
-        for part in (0, half_rows):
-            factor = sum(dot(v[:, part : part + half_rows], eighth, ((0,), (0,))) for v in factors)
-            out[pl.ds(part, half_rows), :] = SS[pl.ds(part, half_rows), :] * factor
+        factors = lax.rsqrt(squares * (1.0 / d_model) + EPS)
+        for b in range(rows // 128):
+            part = pl.ds(b * 128, 128)
+            factor = sum(
+                dot(v, ones, ((0,), (0,))) for v in in_two(jnp.where(row == b, factors, 0.0))
+            )
+            out[part, :] = (SS[part, :] * factor * fin[...]).astype(BF)
     with jax.named_scope("drain"):
         for i, st in enumerate(streams):
             sent(others(st["sizes"][0] * lanes(i)), zs.at[i])
@@ -491,15 +533,22 @@
         ]
 
     half = n_fs // 2
-    n_streams = 9
-    ring = pltpu.SemaphoreType.DMA((n_streams, 2, half))
+    n_streams = 11
+    ring = pltpu.SemaphoreType.DMA((n_streams, half))
     per_stream = pltpu.SemaphoreType.DMA((n_streams,))
     result = pl.pallas_call(
         functools.partial(kernel, n_fs, n_tp),
-        out_shape=jax.ShapeDtypeStruct((rows, width), F32),
-        in_specs=[any_space] * 8 + [vmem] * 6,
+        out_shape=jax.ShapeDtypeStruct((rows, width), BF),
+        in_specs=[any_space] * 15,
         out_specs=vmem,
         scratch_shapes=[
+            scratch(w_low.shape[1], d_model),
+            scratch(1, d_model, dtype=F32),
+            scratch(*w_lift.shape),
+            scratch(1, DK, dtype=F32),
+            scratch(1, DV, dtype=F32),
+            scratch(1, d_model, dtype=F32),
+            scratch(1, width, dtype=F32),
             scratch(n_tp, rows, width),
             scratch(d_model, 2 * DK + DV),
             scratch(n_fs, ko, 128),
@@ -512,14 +561,14 @@
             scratch(n_tp, rows, width),
             scratch(rows, kd_pad),
             scratch(rows, width, dtype=F32),
-            scratch(n_tp, 8, rows, dtype=F32),
+            scratch(n_tp, 8, 128, dtype=F32),
             scratch(DV, DK, dtype=F32),
             *exchange(),
             *exchange(),
-            pltpu.SemaphoreType.DMA((8,)),
+            pltpu.SemaphoreType.DMA((15,)),
             per_stream, ring, per_stream, per_stream,
             pltpu.SemaphoreType.DMA((5,)),
-            pltpu.SemaphoreType.DMA((54,)),
+            pltpu.SemaphoreType.DMA((61,)),
         ],
         compiler_params=pltpu.CompilerParams(
             collective_id=0, has_side_effects=True, vmem_limit_bytes=67043328
@@ -527,9 +576,9 @@
     )(
         tokens, w_query, w_key, w_value, w_out, w_gate.T, w_up.T, w_down,
         w_low.T, attn_gain.reshape(1, -1), w_lift, decay_bias.reshape(1, -1), head_gain.reshape(1, -1),
-        ffn_gain.reshape(1, -1),
+        ffn_gain.reshape(1, -1), final_gain.reshape(1, -1),
     )
-    return (result * final_gain).astype(BF)
+    return result
 
 
 def solution(mesh):

time: 142 us -> 139 us (0.979)
  Pallas kernels: 140 us -> 137 us
  other arithmetic: 1.79 us -> 0 us
  local copies, waits for them, and re-layouts: 0 us -> 1.67 us
    pallas_call x1, Pallas kernels: 140 us -> 137 us  [body(): pl.pallas_call(functools.partial(kernel, n_fs, n_tp), out_shape=jax.Shape...]
    convert_element_type x1 -> x0, other arithmetic: 1.79 us -> none  [body(): return (result * final_gain).astype(BF)]
    unnamed x0 -> x1, local copies, waits for them, and re-layouts: none -> 1.67 us
where the time goes in v3:
time: 139 us
  Pallas kernels  137 us (99%)
  local copies, waits for them, and re-layouts  1.67 us (1%)
    pallas_call x1, Pallas kernels, body(): pl.pallas_call(functools.partial(kernel, n_fs, n_tp), out_shape=jax.Shape...  137 us

profile of v3, /device:TPU:33, one launch (start us, length us, event | category | flops | bytes accessed | tf_op | source)
XLA Modules:
  0.0 138.5 jit_solution(15185092021725757125)
XLA Ops:
  0.0 136.9 %shard_map.145 = bf16[512,256]{1,0:T(8,128)(2,1)} custom-call(bf16[512,256]{1,0:T(8,128)(2,1)} %tok.1, bf16[128,128]{1,0:T(8,128)(2,1)} %wq.1, bf16[128,128]{1,0:T(8,128)(2,1)} %wk.1, bf16[128,256]{1,0:T(8,128)(2,1)} %wv.1, bf16[256,128]{1,0:T(8,128)(2,1)} %wo.1, bf16[704,128]{1,0:T(8,128)(2,1)} %bitcast.8, bf16[704,128]{1,0:T(8,128)(2,1)} %bitcast.9, ...), custom_call_target="tpu_custom_call" | custom-call | tf_op jit(solution)/shard_map/pallas_call | solution.py:539
  136.9 1.7 %copy.17 = bf16[512,256]{1,0:T(8,128)(2,1)} copy(bf16[512,256]{1,0:T(8,128)(2,1)} %shard_map.145) | data formatting | bytes 524288

commit v4 on v3

--- a/solution.py
+++ b/solution.py
@@ -127,15 +127,15 @@
     streams = [
         by_rows(view_q, 0, half_q, 16),
         by_rows(view_q, half_q, half_q, 32),
-        by_rows(view_of(Go), 0, ko, 80),
-        by_rows(view_of(Gg), 0, 256, 80),
-        by_rows(view_of(Gg), units, 256, 80),
-        by_rows(view_of(Gg), 256, 256, 80),
-        by_rows(view_of(Gg), units + 256, 256, 80),
-        by_rows(view_of(Gg), 512, tail, 80),
-        by_rows(view_of(Gg), units + 512, tail, 80),
-        by_rows(view_of(Gd), 0, half_d, 96),
-        by_rows(view_of(Gd), half_d, half_d, 96),
+        by_rows(view_of(Go), 0, ko, 96),
+        by_rows(view_of(Gg), 0, 256, 112),
+        by_rows(view_of(Gg), units, 256, 112),
+        by_rows(view_of(Gg), 256, 256, 112),
+        by_rows(view_of(Gg), units + 256, 256, 112),
+        by_rows(view_of(Gg), 512, tail, tail // 32 * 16),
+        by_rows(view_of(Gg), units + 512, tail, tail // 32 * 16),
+        by_rows(view_of(Gd), 0, half_d, 0),
+        by_rows(view_of(Gd), half_d, half_d, 0),
     ]
     QA, QB, OS, G0, U0, G1, U1, G2, U2, E0, E1 = range(11)
 
@@ -153,7 +153,7 @@
                 ref = st["ring"](shard) if s + 1 < half else st["halves"][way](shard)
                 send(ref, ref, zs.at[i], zr.at[i, s], device)
         for way, (shard, device) in enumerate(flows):
-            if s < half or way == 1:
+            if st["sizes"][1] and (s < half or way == 1):
                 ref = st["mine"](shard)
                 send(ref, ref, ys.at[i], yr.at[i], partner)
 
@@ -168,7 +168,8 @@
 
     def imported(*which):
         for i in which:
-            arrived(others(streams[i]["sizes"][1] * lanes(i)), yr.at[i])
+            if streams[i]["sizes"][1]:
+                arrived(others(streams[i]["sizes"][1] * lanes(i)), yr.at[i])
 
     queue = []
 
@@ -266,11 +267,19 @@
         def quarter(q):
             return pl.ds(q * (half_rows // 2), half_rows // 2)
 
-        def s0(k):
+        def s0(k, late=None):
             slot = other((o_slot, r_slot, l_slot, me)[k])
-            for part in (top, low):
-                PB[k, part, :] = product(slot, part).astype(BF)
-            go(k, PB.at[k], D.at[k], sib)
+
+            def body():
+                for part in (top, low):
+                    PB[k, part, :] = product(slot, part).astype(BF)
+                go(k, PB.at[k], D.at[k], sib)
+
+            if late is None:
+                body()
+            else:
+                last = lax.div(lax.rem(z + half, n_fs), 2)
+                pl.when((slot == last) if late else (slot != last))(body)
 
         def s1(k):
             slot = (o_slot, r_slot, l_slot, me)[k]
@@ -399,15 +408,23 @@
             stage()
             work(0.1)
 
-    def scatter(stages):
+    def scatter(stages, early=False):
         s0, s1, s2, s3, own = stages
-        for k in range(3):
-            s0(k)
-            work(0.25)
-        begun = clock[0] + 0.3
-        s1(0)
-        s0(3)
-        work(0.6)
+        if early:
+            for k in range(4):
+                s0(k, late=False)
+            due(10000.0)
+            for k in range(4):
+                s0(k, late=True)
+            s1(0)
+        else:
+            for k in range(3):
+                s0(k)
+                work(0.25)
+            s1(0)
+            s0(3)
+            work(0.6)
+        begun = clock[0] - 0.3
         for k in range(1, 4):
             s1(k)
             work(0.27)
@@ -435,7 +452,7 @@
         decay(t)
         work(0.6)
     due_to(QB, half)
-    due(clock[0] + 3.0)
+    due(clock[0] + 7.0)
     imported(QA, QB)
     for t in range(4):
         project(t)
@@ -467,10 +484,7 @@
     imported(G2, U2)
     for t in range(2):
         feed(t, 512, units - 512)
-    clock[0] += 2.3
-    due(10000.0)
-    imported(E0, E1)
-    own = scatter(scatter_stages(H, Gd, PB2, D2, S2, B2, A2, T2, SS, 40, 3))
+    own = scatter(scatter_stages(H, Gd, PB2, D2, S2, B2, A2, T2, SS, 40, 3), early=True)
 
     ones = jnp.ones((8, width), BF)
     row = lax.broadcasted_iota(jnp.int32, (8, 128), 0)
@@ -507,7 +521,8 @@
     with jax.named_scope("drain"):
         for i, st in enumerate(streams):
             sent(others(st["sizes"][0] * lanes(i)), zs.at[i])
-            sent(others(st["sizes"][1] * lanes(i)), ys.at[i])
+            if st["sizes"][1]:
+                sent(others(st["sizes"][1] * lanes(i)), ys.at[i])
         for family in range(4):
             sent(X.at[pl.ds(0, n_tp - 1)], xs.at[family])
         sent(Q.at[pl.ds(0, n_tp - 1)], xs.at[4])

time: 139 us -> 135 us (0.971)
  Pallas kernels: 137 us -> 133 us
    pallas_call x1, Pallas kernels: 137 us -> 133 us  [body(): pl.pallas_call(functools.partial(kernel, n_fs, n_tp), out_shape=jax.Shape...]
where the time goes in v4:
time: 135 us
  Pallas kernels  133 us (99%)
  local copies, waits for them, and re-layouts  1.67 us (1%)
    pallas_call x1, Pallas kernels, body(): pl.pallas_call(functools.partial(kernel, n_fs, n_tp), out_shape=jax.Shape...  133 us

profile of v4, /device:TPU:33, one launch (start us, length us, event | category | flops | bytes accessed | tf_op | source)
XLA Modules:
  0.0 135.1 jit_solution(108055171973844190)
XLA Ops:
  0.0 133.4 %shard_map.145 = bf16[512,256]{1,0:T(8,128)(2,1)} custom-call(bf16[512,256]{1,0:T(8,128)(2,1)} %tok.1, bf16[128,128]{1,0:T(8,128)(2,1)} %wq.1, bf16[128,128]{1,0:T(8,128)(2,1)} %wk.1, bf16[128,256]{1,0:T(8,128)(2,1)} %wv.1, bf16[256,128]{1,0:T(8,128)(2,1)} %wo.1, bf16[704,128]{1,0:T(8,128)(2,1)} %bitcast.8, bf16[704,128]{1,0:T(8,128)(2,1)} %bitcast.9, ...), custom_call_target="tpu_custom_call" | custom-call | tf_op jit(solution)/shard_map/pallas_call | solution.py:554
  133.4 1.7 %copy.17 = bf16[512,256]{1,0:T(8,128)(2,1)} copy(bf16[512,256]{1,0:T(8,128)(2,1)} %shard_map.145) | data formatting | bytes 524288

commit v5 on v4

--- a/solution.py
+++ b/solution.py
@@ -225,31 +225,25 @@
         def s1():
             got(0, l_slot, top)
             go(5, l_slot, top, right)
-            go(6, l_slot, top, sib)
+            go(4, l_slot, top, sib)
             got(2, r_slot, low)
-            go(7, r_slot, low, left)
-            go(8, r_slot, low, sib)
+            go(6, r_slot, low, left)
+            go(4, r_slot, low, sib)
 
         def s2():
             got(1, l_slot, low)
-            go(9, l_slot, low, sib)
+            go(4, l_slot, low, sib)
             got(3, r_slot, top)
-            go(10, r_slot, top, sib)
+            go(4, r_slot, top, sib)
 
         def s3():
             got(5, o_slot, top)
-            go(11, o_slot, top, sib)
-            got(7, o_slot, low)
-            go(12, o_slot, low, sib)
+            go(4, o_slot, top, sib)
+            got(6, o_slot, low)
+            go(4, o_slot, low, sib)
 
         def s4():
-            got(4, other(me), None)
-            got(6, other(l_slot), top)
-            got(8, other(r_slot), low)
-            got(9, other(l_slot), low)
-            got(10, other(r_slot), top)
-            got(11, other(o_slot), top)
-            got(12, other(o_slot), low)
+            arrived(buf.at[pl.ds(0, n_tp // 2)], xr.at[base + 4])
 
         return s0, s1, s2, s3, s4
 
@@ -292,14 +286,14 @@
                 for h in range(2):
                     for way in range(2):
                         src = S.at[0, quarter(2 * way + h), :]
-                        go((4, 10, 5, 11)[2 * way + h], src, A.at[way, quarter(h), :], (right, left)[way])
+                        go((4, 5, 6, 7)[2 * way + h], src, A.at[way, quarter(h), :], (right, left)[way])
             elif k == 1:
                 S[1, low, :] = parts[1].astype(BF)
-                go(6, S.at[1, low, :], B.at[0, low, :], right)
+                go(8, S.at[1, low, :], B.at[0, low, :], right)
                 T[0] = parts[0]
             elif k == 2:
                 S[2, top, :] = parts[0].astype(BF)
-                go(7, S.at[2, top, :], B.at[1, top, :], left)
+                go(8, S.at[2, top, :], B.at[1, top, :], left)
                 T[1] = parts[1]
             else:
                 SS[top, :] = parts[0]
@@ -308,15 +302,12 @@
         def s2(h):
             for way in range(2):
                 q = quarter(2 * way + h)
-                got((4, 10, 5, 11)[2 * way + h], A.at[way, quarter(h), :])
+                got((4, 5, 6, 7)[2 * way + h], A.at[way, quarter(h), :])
                 S[1 + way, q, :] = (T[way, quarter(h), :] + A[way, quarter(h), :].astype(F32)).astype(BF)
-                go((8, 12, 9, 13)[2 * way + h], S.at[1 + way, q, :], B.at[way, q, :], (right, left)[way])
+                go(8, S.at[1 + way, q, :], B.at[way, q, :], (right, left)[way])
 
         def s3():
-            got(6, B.at[0, low, :])
-            got(7, B.at[1, top, :])
-            for k, way, q in ((8, 0, 0), (9, 1, 2), (12, 0, 1), (13, 1, 3)):
-                got(k, B.at[way, quarter(q), :])
+            got(8, B)
 
         def own(r):
             return SS[r, :] + B[0, r, :].astype(F32) + B[1, r, :].astype(F32)
@@ -461,7 +452,7 @@
         attend(t)
         work(0.2)
     imported(OS)
-    own = scatter(scatter_stages(M, Go, PB1, D1, S1, B1, A1, T1, SS, 13, 1))
+    own = scatter(scatter_stages(M, Go, PB1, D1, S1, B1, A1, T1, SS, 7, 1))
 
     @pl.loop(0, rows // 64)
     def _(t):
@@ -469,7 +460,7 @@
         F[me, r, :] = (X[me, r, :].astype(F32) + own(r)).astype(BF)
 
     work(0.3)
-    gather(F, 27, 2)
+    gather(F, 16, 2)
     for t in range(4):
         normalize(F, fg, t)
         work(0.55)
@@ -484,7 +475,7 @@
     imported(G2, U2)
     for t in range(2):
         feed(t, 512, units - 512)
-    own = scatter(scatter_stages(H, Gd, PB2, D2, S2, B2, A2, T2, SS, 40, 3), early=True)
+    own = scatter(scatter_stages(H, Gd, PB2, D2, S2, B2, A2, T2, SS, 23, 3), early=True)
 
     ones = jnp.ones((8, width), BF)
     row = lax.broadcasted_iota(jnp.int32, (8, 128), 0)
@@ -504,9 +495,8 @@
         Q[me] = packed
     with jax.named_scope("squares"):
         for k in (4, 5, 3, 2, 6, 7, 1):
-            send(Q.at[me], Q.at[me], xs.at[4], xr.at[53 + k], {"tp": at_tp(k)})
-        for k in range(1, n_tp):
-            arrived(Q.at[at_tp(-k)], xr.at[53 + k])
+            send(Q.at[me], Q.at[me], xs.at[4], xr.at[32], {"tp": at_tp(k)})
+        arrived(Q.at[pl.ds(0, n_tp - 1)], xr.at[32])
     with jax.named_scope("close"):
         squares = Q[0]
         for j in range(1, n_tp):
@@ -583,7 +573,7 @@
             pltpu.SemaphoreType.DMA((15,)),
             per_stream, ring, per_stream, per_stream,
             pltpu.SemaphoreType.DMA((5,)),
-            pltpu.SemaphoreType.DMA((61,)),
+            pltpu.SemaphoreType.DMA((33,)),
         ],
         compiler_params=pltpu.CompilerParams(
             collective_id=0, has_side_effects=True, vmem_limit_bytes=67043328

time: 135 us -> 135 us (level)
  no operation moved by 1% of the time
where the time goes in v5:
time: 135 us
  Pallas kernels  133 us (99%)
  local copies, waits for them, and re-layouts  1.67 us (1%)
    pallas_call x1, Pallas kernels, body(): pl.pallas_call(functools.partial(kernel, n_fs, n_tp), out_shape=jax.Shape...  133 us

profile of v5, /device:TPU:33, one launch (start us, length us, event | category | flops | bytes accessed | tf_op | source)
XLA Modules:
  0.0 134.9 jit_solution(1163830358280029506)
XLA Ops:
  0.0 133.2 %shard_map.145 = bf16[512,256]{1,0:T(8,128)(2,1)} custom-call(bf16[512,256]{1,0:T(8,128)(2,1)} %tok.1, bf16[128,128]{1,0:T(8,128)(2,1)} %wq.1, bf16[128,128]{1,0:T(8,128)(2,1)} %wk.1, bf16[128,256]{1,0:T(8,128)(2,1)} %wv.1, bf16[256,128]{1,0:T(8,128)(2,1)} %wo.1, bf16[704,128]{1,0:T(8,128)(2,1)} %bitcast.8, bf16[704,128]{1,0:T(8,128)(2,1)} %bitcast.9, ...), custom_call_target="tpu_custom_call" | custom-call | tf_op jit(solution)/shard_map/pallas_call | solution.py:544
  133.2 1.7 %copy.17 = bf16[512,256]{1,0:T(8,128)(2,1)} copy(bf16[512,256]{1,0:T(8,128)(2,1)} %shard_map.145) | data formatting | bytes 524288
